TPU v7x, 256 devices: a whole 4x4x8 slice. The times are simulated.
256 devices in a mesh: sp: 16 (over y, x), tp: 16 (over z, core).
Axes of the slice: x: 4, y: 4, z: 8, core: 2. Of those that a mesh axis runs over, the one named last changes fastest.
Arguments:
- conv_outer: bfloat16 [2048, 4096], P('tp', 'sp'), may hold values from -6 to 6
- conv_inner: bfloat16 [2048, 4096], P('tp', 'sp'), may hold values from -6 to 6
- conv_input: bfloat16 [2048, 4096], P('tp', 'sp'), may hold values from -6 to 6
- conv_taps: float32 [3, 2048], P(None, 'tp'), may hold values from -3 to 3
- out_proj: bfloat16 [2048, 4096], P('tp'), may hold values from -0.125 to 0.125
- mixed_state: bfloat16 [4096, 4096], P('sp', 'tp'), may hold values from -6 to 6
- route_ids: int32 [4096, 2], P('sp'), may hold values from 0 to 15, all different within a row; in each aligned block of 256 rows (0 to 255, 256 to 511, ...) at most 64 rows name the same one
- route_weights: float32 [4096, 2], P('sp'), may hold values from 0.1 to 1
- w_gate: bfloat16 [16, 2048, 4096], P('sp', 'tp'), may hold values from -0.09375 to 0.09375
- w_up: bfloat16 [16, 2048, 4096], P('sp', 'tp'), may hold values from -0.09375 to 0.09375
- w_down: bfloat16 [16, 2048, 4096], P('sp', 'tp'), may hold values from -0.125 to 0.125
- cotangent: bfloat16 [4096, 4096], P('sp', 'tp'), may hold values from -8 to 8
Outputs:
- grad_gate: float32 [16, 2048, 4096], P('sp', 'tp')
- grad_up: float32 [16, 2048, 4096], P('sp', 'tp')
- grad_down: float32 [16, 2048, 4096], P('sp', 'tp')
- grad_mixed: bfloat16 [4096, 4096], P('sp', 'tp')
- grad_proj: float32 [2048, 4096], P('tp', 'sp')
- grad_outer: bfloat16 [2048, 4096], P('tp', 'sp')
- grad_inner: bfloat16 [2048, 4096], P('tp', 'sp')
- grad_input: bfloat16 [2048, 4096], P('tp', 'sp')
Inputs may be any that keep to these rules, and one draw needn't show every extreme that they name: `route_ids`: each row names 2 different experts; among the tokens of one index of sp no expert is named more than 64 times, a bound that some block reaches.
All inputs are finite; a program needn't handle non-finite values.
Results may differ from a plain program's by a relative error of at most 0.022.
Values may be sent and summed in bfloat16 or wider, within the bound.
A program may use at most 128 MiB of HBM per device.

v0:
```python
import jax
import jax.numpy as jnp
from jax import lax
from jax.sharding import Mesh
from jax.sharding import PartitionSpec as P

TP = ("tp_0", "tp_1")


def sent_together(arrays, axis, split_dim, concat_dim, along):
    both = jnp.concatenate(arrays, axis=along)
    whole, at, finished = (
        lax.all_to_all(both, axis, split_axis=split_dim, concat_axis=concat_dim, tiled=True),
        0,
        [],
    )
    for a in arrays:
        finished.append(lax.slice_in_dim(whole, at, at + a.shape[along], axis=along))
        at += a.shape[along]
    return tuple(finished)


def in_one_piece(arrays, axis, dim, along):
    both = jnp.concatenate(arrays, axis=along)
    whole, at, finished = (lax.all_gather(both, axis, axis=dim, tiled=True), 0, [])
    for a in arrays:
        finished.append(lax.slice_in_dim(whole, at, at + a.shape[along], axis=along))
        at += a.shape[along]
    return tuple(finished)


def from_behind(value, axis, steps):
    count = lax.axis_size(axis)
    first, last = (max(0, -steps), min(count, count - steps))
    return lax.ppermute(value, axis, [(source, source + steps) for source in range(first, last)])


def whole_of(shard, axes, dim):
    for axis in reversed(axes):
        shard = lax.all_gather(shard, axis, axis=dim, tiled=True)
    return shard


def split_up(shard, dim, size):
    shape = shard.shape
    blocks = shard.reshape(*shape[:dim], size, shape[dim] // size, *shape[dim + 1 :])
    return jnp.moveaxis(blocks, dim, 0)


def summed_on_arrival(shard, axis, dim):
    size = lax.axis_size(axis)
    blocks = lax.all_to_all(split_up(shard, dim, size), axis, 0, 0, tiled=True)
    return jnp.sum(blocks.astype(jnp.float32), axis=0)


def expert_step(rows_in, rows_grad, gate_w, up_w, down_w):
    gate_pre = jnp.einsum("rd,fd->rf", rows_in, gate_w, preferred_element_type=jnp.float32)
    up_pre = jnp.einsum("rd,fd->rf", rows_in, up_w, preferred_element_type=jnp.float32)
    sig_gate = jax.nn.sigmoid(gate_pre)
    silu_gate = gate_pre * sig_gate
    hidden = (silu_gate * up_pre).astype(jnp.bfloat16)
    back_hidden = jnp.einsum("rd,fd->rf", rows_grad, down_w, preferred_element_type=jnp.float32)
    back_gate = (back_hidden * up_pre * sig_gate * (1.0 + gate_pre * (1.0 - sig_gate))).astype(
        jnp.bfloat16
    )
    back_up = (back_hidden * silu_gate).astype(jnp.bfloat16)
    grad_down_e = jnp.einsum("rf,rd->fd", hidden, rows_grad, preferred_element_type=jnp.float32)
    grad_gate_e = jnp.einsum("rf,rd->fd", back_gate, rows_in, preferred_element_type=jnp.float32)
    grad_up_e = jnp.einsum("rf,rd->fd", back_up, rows_in, preferred_element_type=jnp.float32)
    partial_value = jnp.dot(back_gate, gate_w, preferred_element_type=jnp.float32) + jnp.dot(
        back_up, up_w, preferred_element_type=jnp.float32
    )
    return (partial_value, grad_gate_e, grad_up_e, grad_down_e)


def shards(
    conv_outer,
    conv_inner,
    conv_input,
    conv_taps,
    out_proj,
    mixed_state,
    route_ids,
    route_weights,
    w_gate,
    w_up,
    w_down,
    cotangent,
):
    tok_count = mixed_state.shape[0]
    col_count = mixed_state.shape[1]
    top_count = route_ids.shape[1]
    sp_size = lax.axis_size("sp")
    local_experts = w_gate.shape[0]
    experts = local_experts * sp_size
    capacity = 4 * tok_count // experts
    flat_ids = route_ids.reshape(-1)
    onehot = (flat_ids[:, None] == jnp.arange(experts, dtype=jnp.int32)[None, :]).astype(jnp.int32)
    slot_pos = jnp.sum(jnp.cumsum(onehot, axis=0) * onehot, axis=1) - 1
    slot_dest = flat_ids * capacity + slot_pos
    token_of = jnp.arange(flat_ids.shape[0], dtype=jnp.int32) // top_count
    scale_flat = route_weights.reshape(-1)[:, None]

    def pack_rows(rows):
        buffer = jnp.zeros((experts * capacity, rows.shape[1]), rows.dtype).at[slot_dest].set(rows)
        return buffer.reshape(sp_size, local_experts, capacity, rows.shape[1])

    sent_state = pack_rows(mixed_state[token_of])
    sent_grad = pack_rows(
        (cotangent[token_of].astype(jnp.float32) * scale_flat).astype(jnp.bfloat16)
    )
    recv_state, recv_grad = sent_together((sent_state, sent_grad), "sp", 0, 0, 1)
    state_rows, grad_rows = in_one_piece((recv_state[:, 0], recv_grad[:, 0]), TP, 2, 0)
    width = state_rows.shape[2]
    rows_in = state_rows.reshape(-1, width)
    rows_grad = grad_rows.reshape(-1, width)
    partial_value, grad_gate_e, grad_up_e, grad_down_e = expert_step(
        rows_in, rows_grad, w_gate[0], w_up[0], w_down[0]
    )
    summed = lax.psum_scatter(
        partial_value.astype(jnp.bfloat16), TP, scatter_dimension=1, tiled=True
    )
    back_rows = summed.reshape(sp_size, capacity, col_count)
    arrived = lax.all_to_all(
        back_rows[:, None], "sp", split_axis=0, concat_axis=0, tiled=True
    ).reshape(experts * capacity, col_count)
    picked = arrived[slot_dest].astype(jnp.float32).reshape(tok_count, top_count, col_count)
    grad_mixed = (cotangent.astype(jnp.float32) + jnp.sum(picked, axis=1)).astype(jnp.bfloat16)
    taps_count = conv_taps.shape[0]
    rim_width = taps_count - 1
    head_block = from_behind(
        jnp.stack([conv_inner[:, tok_count - rim_width :], conv_input[:, tok_count - rim_width :]]),
        "sp",
        1,
    )
    inner_ext = jnp.concatenate([head_block[0], conv_inner], axis=1).astype(jnp.float32)
    input_ext = jnp.concatenate([head_block[1], conv_input], axis=1).astype(jnp.float32)
    inner_prod = inner_ext * input_ext
    conv_out = jnp.zeros((conv_inner.shape[0], tok_count), jnp.float32)
    for offset in range(taps_count):
        conv_out = (
            conv_out + conv_taps[offset][:, None] * inner_prod[:, offset : offset + tok_count]
        )
    outer_f = conv_outer.astype(jnp.float32)
    mixer_act = (outer_f * conv_out).astype(jnp.bfloat16)
    full_back = whole_of(grad_mixed, TP, 1)
    back_mixer = jnp.einsum("cd,td->ct", out_proj, full_back, preferred_element_type=jnp.float32)
    proj_term = jnp.dot(mixer_act, full_back, preferred_element_type=jnp.float32)
    grad_proj = summed_on_arrival(proj_term.astype(jnp.bfloat16), "sp", 1)
    grad_outer = (back_mixer * conv_out).astype(jnp.bfloat16)
    back_conv = back_mixer * outer_f
    tail_back = from_behind(back_conv[:, :rim_width], "sp", -1)
    back_ext = jnp.concatenate([back_conv, tail_back], axis=1)
    back_prod = jnp.zeros_like(back_conv)
    for offset in range(taps_count):
        shift_by = rim_width - offset
        back_prod = (
            back_prod + conv_taps[offset][:, None] * back_ext[:, shift_by : shift_by + tok_count]
        )
    grad_inner = (back_prod * conv_input.astype(jnp.float32)).astype(jnp.bfloat16)
    grad_input = (back_prod * conv_inner.astype(jnp.float32)).astype(jnp.bfloat16)
    return (
        grad_gate_e[None],
        grad_up_e[None],
        grad_down_e[None],
        grad_mixed,
        grad_proj,
        grad_outer,
        grad_inner,
        grad_input,
    )


def solution(mesh):
    torus = Mesh(mesh.devices.reshape(mesh.shape["sp"], 8, 2), ("sp", "tp_0", "tp_1"))
    return jax.shard_map(
        shards,
        mesh=torus,
        in_specs=(
            P(TP, "sp"),
            P(TP, "sp"),
            P(TP, "sp"),
            P(None, TP),
            P(TP, None),
            P("sp", TP),
            P("sp", None),
            P("sp", None),
            P("sp", TP, None),
            P("sp", TP, None),
            P("sp", TP, None),
            P("sp", TP),
        ),
        out_specs=(
            P("sp", TP, None),
            P("sp", TP, None),
            P("sp", TP, None),
            P("sp", TP),
            P(TP, "sp"),
            P(TP, "sp"),
            P(TP, "sp"),
            P(TP, "sp"),
        ),
        check_vma=False,
    )
```

profile of v0, /device:TPU:17, one launch (start us, length us, event | category | flops | bytes accessed | tf_op | source)
XLA Modules:
  0.0 339.9 jit_solution(3194688719886497391)
XLA Ops:
  8.0 0.8 copy.46
  9.4 1.2 reduce-window.6
  10.9 0.8 copy.49
  11.9 5.8 %scatter_custom_fusion = bf16[1024,256]{1,0:T(8,128)(2,1)S(1)} fusion(s32[512]{0:T(512)S(1)} %bitcast.100, bf16[256,256]{1,0:T(8,128)(2,1)} %param.17, s32[1024]{0:T(1024)S(1)} %pad_clamp_fusion.1, bf16[]{:T(256)} %constant.27.clone.1), kind=kCustom, calls=%fused_computation.33 | custom fusion | bytes 524800 | tf_op jit(solution)/shard_map/scatter | solution.py:105
  17.7 5.9 %scatter_custom_fusion.1 = bf16[1024,256]{1,0:T(8,128)(2,1)S(1)} fusion(s32[512]{0:T(512)S(1)} %bitcast.101, f32[512]{0:T(512)S(1)} %mul.120, bf16[]{:T(256)} %constant.27.clone.1, bf16[256,256]{1,0:T(8,128)(2,1)} %param.23, s32[1024]{0:T(1024)S(1)} %pad_clamp_fusion.1), kind=kCustom, calls=%fused_computation.32 | custom fusion | flops 393216 | bytes 661506 | tf_op jit(solution)/shard_map/scatter | solution.py:105
  23.7 20.9 %all_to_all.15 = bf16[16,2,64,256]{3,2,1,0:T(8,128)(2,1)S(1)} all-to-all(bf16[16,2,64,256]{3,2,1,0:T(8,128)(2,1)S(1)} %pad_maximum_fusion), channel_id=1, replica_groups=mesh['sp'=16,'tp_0'=8,'tp_1'=2] {'sp'}, dimensions={0} | all-to-all | bytes 2097152 | tf_op jit(solution)/shard_map/all_to_all | solution.py:13
  44.6 1.1 pad_maximum_fusion.1
  45.9 104.0 %all-gather.3.cloned.1.call-done = bf16[32,64,4096]{2,1,0:T(8,128)(2,1)} async-done(((bf16[32,64,256]{2,1,0:T(8,128)(2,1)}), bf16[32,64,4096]{2,1,0:T(8,128)(2,1)}) %all-gather.3.cloned.1.call-update) | async-done | bytes 16777232 | tf_op jit(solution)/shard_map/all_gather | solution.py:25
  149.9 6.9 %fusion.33 = (bf16[16,64,4096]{2,1,0:T(8,128)(2,1)S(1)}, bf16[16,64,4096]{2,1,0:T(8,128)(2,1)S(1)}) fusion(bf16[32,64,4096]{2,1,0:T(8,128)(2,1)} %all-gather.3.cloned.1.call-done), kind=kLoop, calls=%fused_computation.87 | loop fusion | bytes 33554432 | tf_op jit(solution)/shard_map/slice | solution.py:27
  156.8 2.3 fusion.2
  159.2 2.3 fusion.5
  161.5 1.3 copy-done.3
  162.9 2.4 multiply_convert_fusion.1
  165.3 8.1 %fusion = f32[1024,4096]{1,0:T(8,128)} fusion(bf16[1024,128]{1,0:T(8,128)(2,1)S(1)} %get-tuple-element.39, bf16[1,128,4096]{2,1,0:T(8,128)(2,1)S(1)} %copy-done), kind=kOutput, calls=%fused_computation.15 | convolution fusion | flops 1073741824 | bytes 18087936 | tf_op jit(solution)/shard_map/dot_general | solution.py:70
  173.3 11.3 %add_convert_fusion = bf16[1024,4096]{1,0:T(8,128)(2,1)} fusion(f32[1024,4096]{1,0:T(8,128)} %fusion, bf16[1024,128]{1,0:T(8,128)(2,1)S(1)} %get-tuple-element.38, bf16[1,128,4096]{2,1,0:T(8,128)(2,1)S(1)} %copy-done.4), kind=kOutput, calls=%fused_computation.5 | convolution fusion | flops 1082130432 | bytes 26476544 | tf_op jit(solution)/shard_map/dot_general | solution.py:70
  184.7 65.8 %reduce-scatter.2.cloned.1.call-done = bf16[1024,256]{1,0:T(8,128)(2,1)} async-done(((bf16[1024,4096]{1,0:T(8,128)(2,1)}), bf16[1024,256]{1,0:T(8,128)(2,1)}) %reduce-scatter.2.cloned.1.call-update) | async-done | bytes 524304 | tf_op jit(solution)/shard_map/reduce_scatter | solution.py:120
  250.5 6.7 %all-to-all-start.1 = ((bf16[16,1,64,256]{3,2,1,0:T(8,128)(2,1)}), bf16[16,1,64,256]{3,2,1,0:T(8,128)(2,1)S(1)}, u32[]{:S(2)}, u32[]{:S(2)}) async-start(bf16[16,1,64,256]{3,2,1,0:T(8,128)(2,1)} %bitcast.99), calls=%async_computation.2 | async-start | bytes 1048576 | tf_op jit(solution)/shard_map/all_to_all | solution.py:124
  257.3 6.6 %all-to-all-done.1 = bf16[16,1,64,256]{3,2,1,0:T(8,128)(2,1)S(1)} async-done(((bf16[16,1,64,256]{3,2,1,0:T(8,128)(2,1)}), bf16[16,1,64,256]{3,2,1,0:T(8,128)(2,1)S(1)}, u32[]{:S(2)}, u32[]{:S(2)}) %all-to-all-start.1) | async-done | bytes 524320 | tf_op jit(solution)/shard_map/all_to_all | solution.py:124
  263.9 1.9 gather_fusion
  266.8 6.8 %all_gather.10 = bf16[256,512]{1,0:T(8,128)(2,1)} all-gather(bf16[256,256]{1,0:T(8,128)(2,1)S(1)} %add_convert_fusion.1), channel_id=1, replica_groups=mesh['sp'=16,'tp_0'=8,'tp_1'=2] {'tp_1'}, dimensions={1}, use_global_device_ids=true | all-gather | bytes 393216 | tf_op jit(solution)/shard_map/all_gather | solution.py:40
  273.9 2.2 collective-permute-start
  276.2 4.1 %collective-permute-done = bf16[2,128,2]{1,2,0:T(2,128)(2,1)S(1)} collective-permute-done((bf16[2,128,2]{1,2,0:T(2,128)(2,1)S(1)}, bf16[2,128,2]{1,2,0:T(2,128)(2,1)S(1)}, u32[]{:S(2)}, u32[]{:S(2)}) %collective-permute-start) | collective-permute-done | bytes 1056 | tf_op jit(solution)/shard_map/ppermute | solution.py:35
  280.4 6.1 %convolution_bitcast_fusion.2 = f32[1,128,4096]{2,1,0:T(8,128)} fusion(bf16[1024,128]{1,0:T(8,128)(2,1)S(1)} %get-tuple-element.39, bf16[1024,4096]{1,0:T(8,128)(2,1)} %bitcast.91), kind=kOutput, calls=%fused_computation.8 | convolution fusion | flops 1073741824 | bytes 10747904 | tf_op jit(solution)/shard_map/rf,rd->fd/dot_general | solution.py:68
  286.4 6.2 %convolution_bitcast_fusion = f32[1,128,4096]{2,1,0:T(8,128)} fusion(bf16[1024,4096]{1,0:T(8,128)(2,1)} %bitcast.94, f32[1024,128]{1,0:T(8,128)S(1)} %fusion.5, f32[1024,128]{1,0:T(8,128)S(1)} %fusion.2), kind=kOutput, calls=%fused_computation.6 | convolution fusion | flops 1074528256 | bytes 11534336 | tf_op jit(solution)/shard_map/rf,rd->fd/dot_general | solution.py:67
  292.6 15.1 %all-gather.5.cloned.1.call-done = bf16[256,4096]{1,0:T(8,128)(2,1)} async-done(((bf16[256,512]{1,0:T(8,128)(2,1)}), bf16[256,4096]{1,0:T(8,128)(2,1)}) %all-gather.5.cloned.1.call-update) | async-done | bytes 2097168 | tf_op jit(solution)/shard_map/all_gather | solution.py:40
  307.7 2.3 multiply_convert_fusion.8
  310.0 2.1 convolution_convert_fusion
  312.1 1.1 copy.68
  313.1 6.7 %all-to-all-start.2 = ((bf16[16,128,256]{2,1,0:T(8,128)(2,1)}), bf16[16,128,256]{2,1,0:T(8,128)(2,1)S(1)}, u32[]{:S(2)}, u32[]{:S(2)}) async-start(bf16[16,128,256]{2,1,0:T(8,128)(2,1)} %bitcast.88), calls=%async_computation.3 | async-start | bytes 2097152 | tf_op jit(solution)/shard_map/all_to_all | solution.py:52
  319.8 4.4 %collective-permute-start.1 = (f32[128,2]{0,1:T(2,128)S(1)}, f32[128,2]{0,1:T(2,128)S(1)}, u32[]{:S(2)}, u32[]{:S(2)}) collective-permute-start(f32[128,2]{0,1:T(2,128)S(1)} %slice.97), channel_id=1, source_target_pairs={{16,0},{32,16},{48,32},{64,48},{80,64},{96,80},{112,96},{128,112},... | collective-permute-start | bytes 3080 | tf_op jit(solution)/shard_map/ppermute | solution.py:35
  324.3 6.0 %convolution_bitcast_fusion.1 = f32[1,128,4096]{2,1,0:T(8,128)} fusion(bf16[1024,128]{1,0:T(8,128)(2,1)S(1)} %get-tuple-element.38, bf16[1024,4096]{1,0:T(8,128)(2,1)} %bitcast.92), kind=kOutput, calls=%fused_computation.7 | convolution fusion | flops 1073741824 | bytes 10747904 | tf_op jit(solution)/shard_map/rf,rd->fd/dot_general | solution.py:69
  332.6 0.8 convert_reduce_fusion
  (68 shorter events, 6.1 us)
Async XLA Ops:
  7.2 149.7 %copy-start = (bf16[1,128,4096]{2,1,0:T(8,128)(2,1)S(1)}, bf16[1,128,4096]{2,1,0:T(8,128)(2,1)}, u32[]{:S(2)}) copy-start(bf16[1,128,4096]{2,1,0:T(8,128)(2,1)} %param.20) | copy-start | bytes 3145732
  7.2 142.7 %all-gather.3.cloned.1.call-start = ((), (), s32[]{:S(2)}) async-start(), calls=%async_computation.4 | async-start | bytes 17825792 | tf_op jit(solution)/shard_map/all_gather | solution.py:25
  45.7 204.8 %reduce-scatter.2.cloned.1.call-start = ((), (), s32[]{:S(2)}) async-start(), calls=%async_computation.5 | async-start | bytes 8912896 | tf_op jit(solution)/shard_map/reduce_scatter | solution.py:120
  156.8 4.7 %copy-start.2 = (bf16[16,64,4096]{2,1,0:T(8,128)(2,1)}, bf16[16,64,4096]{2,1,0:T(8,128)(2,1)S(1)}, u32[]{:S(2)}) copy-start(bf16[16,64,4096]{2,1,0:T(8,128)(2,1)S(1)} %get-tuple-element.37) | copy-start | bytes 25165828
  156.8 6.1 %copy-start.3 = (bf16[16,64,4096]{2,1,0:T(8,128)(2,1)}, bf16[16,64,4096]{2,1,0:T(8,128)(2,1)S(1)}, u32[]{:S(2)}) copy-start(bf16[16,64,4096]{2,1,0:T(8,128)(2,1)S(1)} %get-tuple-element.36) | copy-start | bytes 25165828
  156.8 2.4 copy-start.4
  159.2 3.7 %copy-start.12 = (bf16[1,128,4096]{2,1,0:T(8,128)(2,1)S(1)}, bf16[1,128,4096]{2,1,0:T(8,128)(2,1)}, u32[]{:S(2)}) copy-start(bf16[1,128,4096]{2,1,0:T(8,128)(2,1)} %param.22) | copy-start | bytes 3145732
  184.7 82.1 %copy-start.7 = (bf16[256,256]{1,0:T(8,128)(2,1)S(1)}, bf16[256,256]{1,0:T(8,128)(2,1)}, u32[]{:S(2)}) copy-start(bf16[256,256]{1,0:T(8,128)(2,1)} %param.23) | copy-start | bytes 393220
  184.7 88.9 %copy-start.8 = (bf16[128,256]{1,0:T(8,128)(2,1)S(1)}, bf16[128,256]{1,0:T(8,128)(2,1)}, u32[]{:S(2)}) copy-start(bf16[128,256]{1,0:T(8,128)(2,1)} %param.13) | copy-start | bytes 196612
  184.7 89.1 %copy-start.9 = (bf16[128,256]{1,0:T(8,128)(2,1)S(1)}, bf16[128,256]{1,0:T(8,128)(2,1)}, u32[]{:S(2)}) copy-start(bf16[128,256]{1,0:T(8,128)(2,1)} %param.14) | copy-start | bytes 196612
  184.7 91.4 %copy-start.11 = (f32[3,128]{1,0:T(4,128)S(1)}, f32[3,128]{1,0:T(4,128)}, u32[]{:S(2)}) copy-start(f32[3,128]{1,0:T(4,128)} %param.15) | copy-start | bytes 4612
  184.7 91.4 %copy-start.10 = (bf16[128,256]{1,0:T(8,128)(2,1)S(1)}, bf16[128,256]{1,0:T(8,128)(2,1)}, u32[]{:S(2)}) copy-start(bf16[128,256]{1,0:T(8,128)(2,1)} %param.12) | copy-start | bytes 196612
  250.5 13.4 %all-to-all-start.1 = ((bf16[16,1,64,256]{3,2,1,0:T(8,128)(2,1)}), bf16[16,1,64,256]{3,2,1,0:T(8,128)(2,1)S(1)}, u32[]{:S(2)}, u32[]{:S(2)}) async-start(bf16[16,1,64,256]{3,2,1,0:T(8,128)(2,1)} %bitcast.99), calls=%async_computation.2 | async-start | bytes 1048576 | tf_op jit(solution)/shard_map/all_to_all | solution.py:124
  257.2 50.5 %all-gather.5.cloned.1.call-start = ((), (), s32[]{:S(2)}) async-start(), calls=%async_computation.6 | async-start | bytes 2359296 | tf_op jit(solution)/shard_map/all_gather | solution.py:40
  266.8 25.8 %copy-start.6 = (bf16[256,256]{1,0:T(8,128)(2,1)}, bf16[256,256]{1,0:T(8,128)(2,1)S(1)}, u32[]{:S(2)}) copy-start(bf16[256,256]{1,0:T(8,128)(2,1)S(1)} %add_convert_fusion.1) | copy-start | bytes 393220
  273.9 6.4 %collective-permute-start = (bf16[2,128,2]{1,2,0:T(2,128)(2,1)S(1)}, bf16[2,128,2]{1,2,0:T(2,128)(2,1)S(1)}, u32[]{:S(2)}, u32[]{:S(2)}) collective-permute-start(bf16[2,128,2]{1,2,0:T(2,128)(2,1)S(1)} %pad_maximum_fusion.3), channel_id=1, source_target_pairs={{0,16},{16,32},{32,48},{48,64},{64,80},{80,96},{96,112},{112,128},... | collective-permute-start | bytes 3080 | tf_op jit(solution)/shard_map/ppermute | solution.py:35
  286.4 21.3 %copy-start.5 = (bf16[128,4096]{1,0:T(8,128)(2,1)S(1)}, bf16[128,4096]{1,0:T(8,128)(2,1)}, u32[]{:S(2)}) copy-start(bf16[128,4096]{1,0:T(8,128)(2,1)} %param.16) | copy-start | bytes 3145732
  313.1 19.4 %all-to-all-start.2 = ((bf16[16,128,256]{2,1,0:T(8,128)(2,1)}), bf16[16,128,256]{2,1,0:T(8,128)(2,1)S(1)}, u32[]{:S(2)}, u32[]{:S(2)}) async-start(bf16[16,128,256]{2,1,0:T(8,128)(2,1)} %bitcast.88), calls=%async_computation.3 | async-start | bytes 2097152 | tf_op jit(solution)/shard_map/all_to_all | solution.py:52
  319.8 13.6 %copy-start.1 = (bf16[1,128,4096]{2,1,0:T(8,128)(2,1)S(1)}, bf16[1,128,4096]{2,1,0:T(8,128)(2,1)}, u32[]{:S(2)}) copy-start(bf16[1,128,4096]{2,1,0:T(8,128)(2,1)} %param.20) | copy-start | bytes 3145732
  319.8 11.2 %collective-permute-start.1 = (f32[128,2]{0,1:T(2,128)S(1)}, f32[128,2]{0,1:T(2,128)S(1)}, u32[]{:S(2)}, u32[]{:S(2)}) collective-permute-start(f32[128,2]{0,1:T(2,128)S(1)} %slice.97), channel_id=1, source_target_pairs={{16,0},{32,16},{48,32},{64,48},{80,64},{96,80},{112,96},{128,112},... | collective-permute-start | bytes 3080 | tf_op jit(solution)/shard_map/ppermute | solution.py:35
Sparse Core Ops, SparseCore 0:
  45.8 104.0 all-gather.2
  184.8 65.6 reduce-scatter.1
  273.7 33.9 all-gather.4
where the time goes:
time: 346 us; the launch traced here: 340 us
  waiting for transfers between devices  196 us (57%)
  matrix products  49 us (14%)
  blocking collectives  27.6 us (8%)
  local copies, waits for them, and re-layouts  22.5 us (7%)
  starting transfers between devices  20.3 us (6%)
  between operations  14.1 us (4%)
  other arithmetic  10.7 us (3%)
    all_gather x1, waiting for transfers between devices, in_one_piece(): lax.all_gather(both, axis, axis=dim, tiled=True)  104 us
    reduce_scatter x1, waiting for transfers between devices, shards(): lax.psum_scatter(partial_value.astype(jnp.bfloat16), TP, scatter_dimensio...  65.8 us
    all_to_all x1, blocking collectives, sent_together(): lax.all_to_all(both, axis, split_axis=split_dim, concat_axis=concat_dim,...  20.9 us
    all_gather x1, waiting for transfers between devices, whole_of(): shard = lax.all_gather(shard, axis, axis=dim, tiled=True)  15.1 us
    dot_general x1, matrix products, expert_step(): jnp.dot(back_up, up_w, preferred_element_type=jnp.float32)  11.3 us
    dot_general x1, matrix products, expert_step(): jnp.dot(back_gate, gate_w, preferred_element_type=jnp.float32)  8.07 us
  transfers between devices with their start and end apart: 7, of which 5 were waited for; matrix products, arithmetic and copies ran while one was open for 6% of the time, Pallas kernels for 0%

commit v1 on v0

v1 whole, which is shorter than its diff:
```python
import functools

import jax
import jax.numpy as jnp
from jax import lax
from jax.experimental import pallas as pl
from jax.experimental.pallas import tpu as pltpu
from jax.sharding import Mesh
from jax.sharding import PartitionSpec as P

BF = jnp.bfloat16
F32 = jnp.float32
MESH_ID = pl.DeviceIdType.MESH
SUBS = 4


def dot(a, b):
    return lax.dot_general(a, b, (((1,), (0,)), ((), ())), preferred_element_type=F32)


def dot_nt(a, b):
    return lax.dot_general(a, b, (((1,), (1,)), ((), ())), preferred_element_type=F32)


def kernel(
    dims,
    ids,
    wts,
    state,
    cot,
    c_outer,
    c_inner,
    c_input,
    taps,
    wg_hbm,
    wu_hbm,
    wd_hbm,
    op_hbm,
    gg_hbm,
    gu_hbm,
    gd_hbm,
    gm_out,
    gproj,
    gouter,
    ginner,
    ginput,
    rows_all,
    wgu,
    wd,
    op,
    sent,
    acc_gu,
    acc_d,
    pick,
    pick_t,
    bgu,
    bgu_t,
    hid_t,
    part_out,
    part_in,
    run,
    back,
    grad_gu,
    grad_d,
    full,
    proj_out,
    proj_in,
    rim_in,
    tail_out,
    tail_in,
    conv_s,
    act_s,
    bm_acc,
    w_sem,
    o_sem,
    a_send,
    a_recv,
    g_send,
    g_recv,
    d_send,
    d_recv,
    p_send,
    p_recv,
    r_send,
    r_recv,
    b_send,
    b_recv,
    f_send,
    f_recv,
    e_send,
    e_recv,
    j_send,
    j_recv,
    h_send,
    h_recv,
    t_send,
    t_recv,
):
    ny, nx, nz = dims
    ns = ny * nx
    hid, d_all = wg_hbm.shape
    toks, feat = state.shape
    cap = sent.shape[2]
    slots = ns * cap
    y, x = lax.axis_index("y"), lax.axis_index("x")
    z, c = lax.axis_index("z"), lax.axis_index("c")
    me = y * nx + x
    other = 1 - c
    up, down = lax.rem(z + 1, nz), lax.rem(z + nz - 1, nz)
    shifts = [(dy, dx) for dy in range(ny) for dx in range(nx) if (dy, dx) != (0, 0)]
    following, previous = lax.rem(me + 1, ns), lax.rem(me + ns - 1, ns)

    def at_plane(dy, dx):
        py, px = lax.rem(y + dy, ny), lax.rem(x + dx, nx)
        return {"y": py, "x": px, "z": z, "c": c}, py * nx + px

    def on_sp(s):
        return {"y": lax.div(s, nx), "x": lax.rem(s, nx), "z": z, "c": c}

    def on_z(pos):
        return {"y": y, "x": x, "z": pos, "c": c}

    partner = {"y": y, "x": x, "z": z, "c": other}

    def remote(src, dst, send, recv, device):
        return pltpu.make_async_remote_copy(
            src_ref=src,
            dst_ref=dst,
            send_sem=send,
            recv_sem=recv,
            device_id=device,
            device_id_type=MESH_ID,
        )

    def cols(index):
        return pl.ds(pl.multiple_of(index * feat, feat), feat)

    loads = [
        pltpu.make_async_copy(wg_hbm, wgu.at[pl.ds(0, hid)], w_sem.at[0]),
        pltpu.make_async_copy(wu_hbm, wgu.at[pl.ds(hid, hid)], w_sem.at[1]),
        pltpu.make_async_copy(wd_hbm, wd, w_sem.at[2]),
        pltpu.make_async_copy(op_hbm, op, w_sem.at[3]),
    ]
    for load in loads:
        load.start()

    barrier = pltpu.get_barrier_semaphore()
    peers = [at_plane(dy, dx)[0] for dy, dx in shifts] + [on_z(up), on_z(down), partner]
    for peer in peers:
        pl.semaphore_signal(barrier, inc=1, device_id=peer, device_id_type=MESH_ID)

    expert = lax.broadcasted_iota(jnp.int32, (ns, toks), 0)
    first, second = ids[0:1, :] == expert, ids[1:2, :] == expert
    named = jnp.where(first, 1.0, 0.0) + jnp.where(second, 1.0, 0.0)
    weight = jnp.where(first, wts[0:1, :], 0.0) + jnp.where(second, wts[1:2, :], 0.0)
    earlier = jnp.where(
        lax.broadcasted_iota(jnp.int32, (toks, toks), 0)
        < lax.broadcasted_iota(jnp.int32, (toks, toks), 1),
        1.0,
        0.0,
    ).astype(BF)
    count = jnp.where(named > 0.0, dot(named.astype(BF), earlier), -1.0)
    place = lax.broadcasted_iota(jnp.int32, (cap, toks), 0).astype(F32)
    scales = []
    for e in range(ns):
        hit = jnp.where(count[e : e + 1, :] == place, 1.0, 0.0)
        pick[pl.ds(e * cap, cap), :] = hit.astype(BF)
        scales.append(jnp.sum(hit * weight[e : e + 1, :], axis=1, keepdims=True))
    scale = jnp.concatenate(scales, axis=0)
    sent[0] = dot(pick[...], state[...]).astype(BF).reshape(ns, cap, feat)
    sent[1] = (dot(pick[...], cot[...]) * scale).astype(BF).reshape(ns, cap, feat)

    pl.semaphore_wait(barrier, len(peers))

    def route_copy(arr, index, dst_z, dev, s_to):
        return remote(
            sent.at[arr, s_to],
            rows_all.at[arr, z, c, me],
            a_send.at[arr, index],
            a_recv.at[arr, me],
            dev,
        )

    def route_wait(arr, s_from):
        remote(
            sent.at[arr, s_from],
            rows_all.at[arr, z, c, s_from],
            a_send.at[arr, 0],
            a_recv.at[arr, s_from],
            partner,
        ).wait_recv()

    for index, (dy, dx) in enumerate(shifts):
        dev, s_to = at_plane(dy, dx)
        for arr in range(2):
            route_copy(arr, index, z, dev, s_to).start()
    for arr in range(2):
        rows_all[arr, z, c, me] = sent[arr, me]

    def rim_copy(arr, dev):
        src = (c_inner, c_input)[arr]
        lanes = src.shape[1]
        return remote(
            src.at[:, pl.ds(lanes - 128, 128)], rim_in.at[arr], h_send.at[arr], h_recv.at[arr], dev
        )

    for arr in range(2):
        rim_copy(arr, on_sp(following)).start()

    acc_gu[...] = jnp.zeros_like(acc_gu)
    acc_d[...] = jnp.zeros_like(acc_d)
    per_sub = ns // SUBS

    def source_of(arr, t):
        return lax.rem(z + nz - t, nz) if arr == 0 else lax.rem(z + t, nz)

    def ring_copy(arr, sub, t):
        part = rows_all.at[arr, source_of(arr, t), c, pl.ds(sub * per_sub, per_sub)]
        return remote(
            part,
            part,
            g_send.at[arr, sub, t],
            g_recv.at[arr, sub, t],
            on_z(up if arr == 0 else down),
        )

    def ring_wait(arr, sub, t):
        part = rows_all.at[arr, source_of(arr, t), c, pl.ds(sub * per_sub, per_sub)]
        remote(
            part, part, g_send.at[arr, sub, t - 1], g_recv.at[arr, sub, t - 1], partner
        ).wait_recv()

    def share(arr, t):
        part = rows_all.at[arr, source_of(arr, t), c]
        return remote(part, part, d_send.at[arr, t], d_recv.at[arr, t], partner)

    def share_wait(arr, t):
        part = rows_all.at[arr, source_of(arr, t), other]
        remote(part, part, d_send.at[arr, t], d_recv.at[arr, t], partner).wait_recv()

    def products(t):
        for arr in range(2):
            share_wait(arr, t)
        for lane in range(2):
            at = source_of(0, t)
            rows = rows_all[0, at, lane].reshape(slots, feat)
            acc_gu[...] += dot_nt(rows, wgu[:, cols(at * 2 + lane)])
            at = source_of(1, t)
            rows = rows_all[1, at, lane].reshape(slots, feat)
            acc_d[...] += dot_nt(rows, wd[:, cols(at * 2 + lane)])

    for sub in range(SUBS):
        for arr in range(2):
            for s_from in range(sub * per_sub, (sub + 1) * per_sub):

                @pl.when(s_from != me)
                def _():
                    route_wait(arr, s_from)

            ring_copy(arr, sub, 0).start()
    for arr in range(2):
        share(arr, 0).start()

    for arr in range(2):
        rim_copy(arr, on_sp(previous)).wait_recv()
    inner, inp = c_inner[...].astype(F32), c_input[...].astype(F32)
    rim_prod = rim_in[0].astype(F32) * rim_in[1].astype(F32)
    rim_prod = jnp.where(me == 0, 0.0, rim_prod)
    ext = jnp.concatenate([rim_prod, inner * inp], axis=1)
    n_taps = taps.shape[1]
    conv_out = taps[:, n_taps - 1 : n_taps] * (inner * inp)
    for j in range(n_taps - 1):
        conv_out = conv_out + taps[:, j : j + 1] * pltpu.roll(ext, n_taps - 1 - j, 1)[:, 128:]
    conv_s[...] = conv_out
    act_s[...] = (c_outer[...].astype(F32) * conv_out).astype(BF)
    pick_t[...] = pick[...].T

    for load in loads:
        load.wait()

    def ring_step(t, carry):
        for sub in range(SUBS):
            for arr in range(2):
                ring_wait(arr, sub, t)

                @pl.when(t < nz - 1)
                def _():
                    ring_copy(arr, sub, t).start()

        for arr in range(2):
            share(arr, t).start()
        products(t - 1)
        return carry

    lax.fori_loop(1, nz, ring_step, 0)
    products(nz - 1)

    gate_pre, up_pre = acc_gu[:, :hid], acc_gu[:, hid:]
    back_hidden = acc_d[...]
    sig = jax.nn.sigmoid(gate_pre)
    silu = gate_pre * sig
    hid_t[...] = (silu * up_pre).astype(BF).T
    back_gate = (back_hidden * up_pre * sig * (1.0 + gate_pre * (1.0 - sig))).astype(BF)
    back_up = (back_hidden * silu).astype(BF)
    bgu[:, :hid] = back_gate
    bgu[:, hid:] = back_up
    bgu_t[:hid, :] = back_gate.T
    bgu_t[hid:, :] = back_up.T

    half = slots // 2
    quarter = half // 2

    def target_of(way, t):
        return lax.rem(z + 2 * nz - 1 - t, nz) if way == 0 else lax.rem(z + 1 + t, nz)

    def part_copy(way, t):
        return remote(
            part_out.at[way, t], part_in.at[way, t], p_send.at[way, t], p_recv.at[way, t], partner
        )

    def partner_part(t):
        for way in range(2):
            w = wgu[:, cols(target_of(way, t) * 2 + other)]
            part_out[way, t] = dot(bgu[pl.ds(way * half, half), :], w).astype(BF)
            part_copy(way, t).start()

    def run_copy(way, sub, t):
        rows = pl.ds(sub * quarter, quarter)
        return remote(
            run.at[way, t, rows],
            run.at[way, t + 1, rows],
            r_send.at[way, sub, t],
            r_recv.at[way, sub, t],
            on_z(up if way == 0 else down),
        )

    for way in range(2):
        run[way, 0] = jnp.zeros((half, feat), BF)
    partner_part(0)

    def reduce_step(t, carry):
        @pl.when(t < nz - 1)
        def _():
            partner_part(t + 1)

        for lane in range(2):
            rows = rows_all[0, t, lane].reshape(slots, feat)
            grad_gu[:, cols(t * 2 + lane)] = dot(bgu_t[...], rows)
            rows = rows_all[1, t, lane].reshape(slots, feat)
            grad_d[:, cols(t * 2 + lane)] = dot(hid_t[...], rows)
        for way in range(2):
            part_copy(way, t).wait_recv()
        for sub in range(2):
            for way in range(2):
                rows = pl.ds(sub * quarter, quarter)

                @pl.when(t > 0)
                def _():
                    run_copy(way, sub, t - 1).wait_recv()

                w = wgu[:, cols(target_of(way, t) * 2 + c)]
                own = dot(bgu[pl.ds(way * half + sub * quarter, quarter), :], w)
                total = own + part_in[way, t, rows].astype(F32) + run[way, t, rows].astype(F32)
                run[way, t, rows] = total.astype(BF)

                @pl.when(t < nz - 1)
                def _():
                    run_copy(way, sub, t).start()

        return carry

    lax.fori_loop(0, nz, reduce_step, 0)

    results = [
        pltpu.make_async_copy(grad_gu.at[pl.ds(0, hid)], gg_hbm, o_sem.at[0]),
        pltpu.make_async_copy(grad_gu.at[pl.ds(hid, hid)], gu_hbm, o_sem.at[1]),
        pltpu.make_async_copy(grad_d, gd_hbm, o_sem.at[2]),
    ]

    def back_src(s):
        way, row = lax.div(s, ns // 2), lax.rem(s, ns // 2)
        return run.at[way, nz - 1, pl.ds(pl.multiple_of(row * cap, cap), cap)]

    def back_copy(index, dev, s_to):
        return remote(back_src(s_to), back.at[me], b_send.at[index], b_recv.at[me], dev)

    for index, (dy, dx) in enumerate(shifts):
        dev, s_to = at_plane(dy, dx)
        back_copy(index, dev, s_to).start()
    back[me] = back_src(me)[...]
    for result in results:
        result.start()
    for dy, dx in shifts:
        _, s_from = at_plane(dy, dx)
        remote(
            back_src(s_from), back.at[s_from], b_send.at[0], b_recv.at[s_from], partner
        ).wait_recv()
    moe = dot(pick_t[...], back[...].reshape(slots, feat))
    grad_mixed = (cot[...].astype(F32) + moe).astype(BF)
    gm_out[...] = grad_mixed
    full[z, c] = grad_mixed

    halves = toks // 2
    hops = {(0, h): nz // 2 - h for h in range(2)} | {(1, h): nz // 2 - 1 + h for h in range(2)}

    def full_part(way, h, k, lane):
        at = lax.rem(z + nz - k, nz) if way == 0 else lax.rem(z + k, nz)
        return full.at[at, lane, pl.ds(h * halves, halves)]

    def full_copy(way, h, k):
        part = full_part(way, h, k, c)
        return remote(
            part, part, f_send.at[way, h, k], f_recv.at[way, h, k], on_z(up if way == 0 else down)
        )

    def full_wait(way, h, k):
        part = full_part(way, h, k, c)
        remote(
            part, part, f_send.at[way, h, k - 1], f_recv.at[way, h, k - 1], partner
        ).wait_recv()

    def full_share(way, h, k, lane):
        part = full_part(way, h, k, lane)
        return remote(part, part, e_send.at[way, h, k], e_recv.at[way, h, k], partner)

    bm_acc[...] = jnp.zeros_like(bm_acc)

    def mixer_products(at):
        for lane in range(2):
            f = full[at, lane]
            bm_acc[...] += dot_nt(op[:, cols(at * 2 + lane)], f)
            proj_out[at * 2 + lane] = dot(act_s[...], f).astype(BF)

    shared = []
    for h in range(2):
        for way in range(2):
            if hops[(way, h)] > 0:
                full_copy(way, h, 0).start()
    for h in range(2):
        full_share(0, h, 0, c).start()
        shared.append((0, h, 0))
    pending = [(0, [(0, 0, 0), (0, 1, 0)])]
    for k in range(1, nz // 2 + 1):
        news = {}
        for h in range(2):
            for way in range(2):
                if k > hops[(way, h)]:
                    continue
                full_wait(way, h, k)
                if k < hops[(way, h)]:
                    full_copy(way, h, k).start()
                full_share(way, h, k, c).start()
                shared.append((way, h, k))
                news.setdefault(k if (way == 0 or 2 * k == nz) else -k, []).append((way, h, k))
        for pos, waits in pending:
            for args in waits:
                full_share(*args, other).wait_recv()
            mixer_products(lax.rem(z + nz - pos, nz))
        pending = list(news.items())
    for pos, waits in pending:
        for args in waits:
            full_share(*args, other).wait_recv()
        mixer_products(lax.rem(z + nz - pos, nz))

    back_mixer = bm_acc[...]
    back_conv = back_mixer * c_outer[...].astype(F32)
    tail_out[...] = back_conv[:, :128]

    def tail_copy(dev):
        return remote(tail_out, tail_in, t_send.at[0], t_recv.at[0], dev)

    tail_copy(on_sp(previous)).start()

    def proj_copy(index, dev, s_to):
        return remote(proj_out.at[s_to], proj_in.at[me], j_send.at[index], j_recv.at[me], dev)

    for index, (dy, dx) in enumerate(shifts):
        dev, s_to = at_plane(dy, dx)
        proj_copy(index, dev, s_to).start()

    gouter[...] = (back_mixer * conv_s[...]).astype(BF)
    tail_copy(on_sp(following)).wait_recv()
    tail = jnp.where(me == ns - 1, 0.0, tail_in[...])
    ext = jnp.concatenate([back_conv, tail], axis=1)
    width = ext.shape[1]
    back_prod = taps[:, n_taps - 1 : n_taps] * back_conv
    for j in range(n_taps - 1):
        back_prod = (
            back_prod + taps[:, j : j + 1] * pltpu.roll(ext, width - (n_taps - 1 - j), 1)[:, :toks]
        )
    ginner[...] = (back_prod * c_input[...].astype(F32)).astype(BF)
    ginput[...] = (back_prod * c_inner[...].astype(F32)).astype(BF)

    proj_total = proj_out[me].astype(F32)
    for dy, dx in shifts:
        _, s_from = at_plane(dy, dx)
        remote(
            proj_out.at[s_from], proj_in.at[s_from], j_send.at[0], j_recv.at[s_from], partner
        ).wait_recv()
        proj_total = proj_total + proj_in[s_from].astype(F32)
    gproj[...] = proj_total

    for result in results:
        result.wait()
    for index, (dy, dx) in enumerate(shifts):
        dev, s_to = at_plane(dy, dx)
        for arr in range(2):
            route_copy(arr, index, z, dev, s_to).wait_send()
        back_copy(index, dev, s_to).wait_send()
        proj_copy(index, dev, s_to).wait_send()
    for arr in range(2):
        rim_copy(arr, on_sp(following)).wait_send()
    tail_copy(on_sp(previous)).wait_send()

    def ring_sent(t, carry):
        for arr in range(2):
            for sub in range(SUBS):
                ring_copy(arr, sub, t).wait_send()
            for sub in range(2):
                run_copy(arr, sub, t).wait_send()
        return carry

    lax.fori_loop(0, nz - 1, ring_sent, 0)

    def shares_sent(t, carry):
        for arr in range(2):
            share(arr, t).wait_send()
            part_copy(arr, t).wait_send()
        return carry

    lax.fori_loop(0, nz, shares_sent, 0)
    for (way, h), n in hops.items():
        for k in range(n):
            full_copy(way, h, k).wait_send()
    for args in shared:
        full_share(*args, c).wait_send()


def shards(
    dims,
    conv_outer,
    conv_inner,
    conv_input,
    conv_taps,
    out_proj,
    mixed_state,
    route_ids,
    route_weights,
    w_gate,
    w_up,
    w_down,
    cotangent,
):
    ny, nx, nz = dims
    ns = ny * nx
    toks, feat = mixed_state.shape
    hid, d_all = out_proj.shape[0], out_proj.shape[1]
    chans = conv_outer.shape[0]
    hid = w_gate.shape[1]
    cap = 4 * toks // ns
    slots = ns * cap
    vmem = pl.BlockSpec(memory_space=pltpu.VMEM)
    hbm = pl.BlockSpec(memory_space=pl.ANY)
    dma = pltpu.SemaphoreType.DMA
    scratch = [
        pltpu.VMEM((2, nz, 2, ns, cap, feat), BF),
        pltpu.VMEM((2 * hid, d_all), BF),
        pltpu.VMEM((hid, d_all), BF),
        pltpu.VMEM((chans, d_all), BF),
        pltpu.VMEM((2, ns, cap, feat), BF),
        pltpu.VMEM((slots, 2 * hid), F32),
        pltpu.VMEM((slots, hid), F32),
        pltpu.VMEM((slots, toks), BF),
        pltpu.VMEM((toks, slots), BF),
        pltpu.VMEM((slots, 2 * hid), BF),
        pltpu.VMEM((2 * hid, slots), BF),
        pltpu.VMEM((hid, slots), BF),
        pltpu.VMEM((2, nz, slots // 2, feat), BF),
        pltpu.VMEM((2, nz, slots // 2, feat), BF),
        pltpu.VMEM((2, nz, slots // 2, feat), BF),
        pltpu.VMEM((ns, cap, feat), BF),
        pltpu.VMEM((2 * hid, d_all), F32),
        pltpu.VMEM((hid, d_all), F32),
        pltpu.VMEM((nz, 2, toks, feat), BF),
        pltpu.VMEM((nz * 2, chans, feat), BF),
        pltpu.VMEM((ns, chans, feat), BF),
        pltpu.VMEM((2, chans, 128), BF),
        pltpu.VMEM((chans, 128), F32),
        pltpu.VMEM((chans, 128), F32),
        pltpu.VMEM((chans, toks), F32),
        pltpu.VMEM((chans, toks), BF),
        pltpu.VMEM((chans, toks), F32),
        dma((4,)),
        dma((3,)),
        dma((2, ns)),
        dma((2, ns)),
        dma((2, SUBS, nz)),
        dma((2, SUBS, nz)),
        dma((2, nz)),
        dma((2, nz)),
        dma((2, nz)),
        dma((2, nz)),
        dma((2, 2, nz)),
        dma((2, 2, nz)),
        dma((ns,)),
        dma((ns,)),
        dma((2, 2, nz)),
        dma((2, 2, nz)),
        dma((2, 2, nz)),
        dma((2, 2, nz)),
        dma((ns,)),
        dma((ns,)),
        dma((2,)),
        dma((2,)),
        dma((1,)),
        dma((1,)),
    ]
    grad = jax.ShapeDtypeStruct((hid, d_all), F32)
    conv = jax.ShapeDtypeStruct((chans, toks), BF)
    outs = pl.pallas_call(
        functools.partial(kernel, dims),
        out_shape=(
            grad,
            grad,
            grad,
            jax.ShapeDtypeStruct((toks, feat), BF),
            jax.ShapeDtypeStruct((chans, feat), F32),
            conv,
            conv,
            conv,
        ),
        in_specs=[vmem] * 8 + [hbm] * 4,
        out_specs=(hbm,) * 3 + (vmem,) * 5,
        scratch_shapes=scratch,
        compiler_params=pltpu.CompilerParams(
            collective_id=0, has_side_effects=True, vmem_limit_bytes=66000000
        ),
    )(
        route_ids.T,
        route_weights.T,
        mixed_state,
        cotangent,
        conv_outer,
        conv_inner,
        conv_input,
        conv_taps.T,
        w_gate[0],
        w_up[0],
        w_down[0],
        out_proj,
    )
    return (outs[0][None], outs[1][None], outs[2][None], *outs[3:])


def solution(mesh):
    dims = (4, 4, 8)
    return on_torus(Mesh(mesh.devices.reshape(*dims, 2), ("y", "x", "z", "c")), dims)


def on_torus(torus, dims):
    sp, tp = ("y", "x"), ("z", "c")
    return jax.shard_map(
        functools.partial(shards, dims),
        mesh=torus,
        in_specs=(
            P(tp, sp),
            P(tp, sp),
            P(tp, sp),
            P(None, tp),
            P(tp, None),
            P(sp, tp),
            P(sp, None),
            P(sp, None),
            P(sp, tp, None),
            P(sp, tp, None),
            P(sp, tp, None),
            P(sp, tp),
        ),
        out_specs=(
            P(sp, tp, None),
            P(sp, tp, None),
            P(sp, tp, None),
            P(sp, tp),
            P(tp, sp),
            P(tp, sp),
            P(tp, sp),
            P(tp, sp),
        ),
        check_vma=False,
    )
```

time: 346 us -> 214 us (0.62)
  Pallas kernels: 0 us -> 199 us
  waiting for transfers between devices: 196 us -> 0 us
  matrix products: 49 us -> 0 us
  blocking collectives: 27.6 us -> 0 us
  starting transfers between devices: 20.3 us -> 0 us
  between operations: 14.1 us -> 0.67 us
  local copies, waits for them, and re-layouts: 22.5 us -> 11.6 us
  other arithmetic: 10.7 us -> 0 us
    pallas_call x0 -> x1, Pallas kernels: none -> 199 us  [shards(): pl.pallas_call(functools.partial(kernel, dims), out_shape=(grad, grad, gr...]
    all_gather x2 -> x0, waiting for transfers between devices: 119 us -> none  [the longest x1 104 us: in_one_piece(): lax.all_gather(both, axis, axis=dim, tiled=True)]
    reduce_scatter x1 -> x0, waiting for transfers between devices: 65.8 us -> none  [shards(): lax.psum_scatter(partial_value.astype(jnp.bfloat16), TP, scatter_dimensio...]
    dot_general x10 -> x0, matrix products: 49 us -> none  [the longest x1 11.3 us: expert_step(): jnp.dot(back_up, up_w, preferred_element_type=jnp.float32)]
    all_to_all x1 -> x0, blocking collectives: 20.9 us -> none  [sent_together(): lax.all_to_all(both, axis, split_axis=split_dim, concat_axis=concat_dim,...]
    all_to_all x2 -> x0, starting transfers between devices: 13.4 us -> none  [the longest x1 6.68 us: shards(): lax.all_to_all(back_rows[:, None], 'sp', split_axis=0, concat_axis=0, til...]
    slice x3 -> x0, local copies, waits for them, and re-layouts: 7.1 us -> none  [the longest x1 6.88 us: in_one_piece(): lax.slice_in_dim(whole, at, at + a.shape[along], axis=along)]
    all_gather x1 -> x0, blocking collectives: 6.77 us -> none  [whole_of(): shard = lax.all_gather(shard, axis, axis=dim, tiled=True)]
  transfers between devices with their start and end apart: 7 -> 0, of which waited for: 5 -> 0; matrix products, arithmetic and copies ran while one was open for 6% -> 0% of each run, Pallas kernels for 0% -> 0%
where the time goes in v1:
time: 214 us; the launch traced here: 211 us
  Pallas kernels  199 us (93%)
  local copies, waits for them, and re-layouts  11.6 us (5%)
    pallas_call x1, Pallas kernels, shards(): pl.pallas_call(functools.partial(kernel, dims), out_shape=(grad, grad, gr...  199 us
    unnamed x23, local copies, waits for them, and re-layouts  11.6 us

profile of v1, /device:TPU:17, one launch (start us, length us, event | category | flops | bytes accessed | tf_op | source)
XLA Modules:
  0.0 211.3 jit_solution(16600653922990946996)
XLA Ops:
  0.6 1.4 copy.20
  2.0 199.0 %shard_map.179 = (f32[128,4096]{1,0:T(8,128)}, f32[128,4096]{1,0:T(8,128)}, f32[128,4096]{1,0:T(8,128)}, bf16[256,256]{1,0:T(8,128)(2,1)}, f32[128,256]{1,0:T(8,...) custom-call(s32[2,256]{1,0:T(2,128)} %bitcast.16, f32[2,256]{1,0:T(2,128)} %bitcast.17, ...), custom_call_target="tpu_custom_call" | custom-call | tf_op jit(solution)/shard_map/pallas_call | solution.py:620
  201.1 0.0 copy-start.1
  201.1 3.3 %copy.29 = f32[1,128,4096]{2,1,0:T(8,128)} copy(f32[1,128,4096]{2,1,0:T(8,128)} %bitcast.11) | data formatting | bytes 4194304
  204.4 0.0 copy-done.1
  204.4 0.0 copy-start
  204.4 1.3 copy.30
  205.7 1.0 copy-done
  206.7 0.0 copy-start.3
  206.7 0.0 copy-start.2
  206.7 0.0 copy-start.6
  206.7 0.0 copy-start.5
  206.7 0.0 copy-start.4
  206.8 1.3 copy.31
  208.1 0.0 copy-done.3
  208.1 0.7 copy.32
  208.7 0.0 copy-done.2
  208.7 0.7 copy.33
  209.4 0.0 copy-done.6
  209.4 0.6 copy.34
  210.0 0.0 copy-done.5
  210.0 0.6 copy.35
  210.7 0.0 copy-done.4
  210.7 0.6 copy.36
Async XLA Ops:
  201.1 3.3 %copy-start.1 = (f32[128,4096]{1,0:T(8,128)S(1)}, f32[128,4096]{1,0:T(8,128)}, u32[]{:S(2)}) copy-start(f32[128,4096]{1,0:T(8,128)} %get-tuple-element.17) | copy-start | bytes 6291460
  204.4 2.3 %copy-start = (f32[128,4096]{1,0:T(8,128)S(1)}, f32[128,4096]{1,0:T(8,128)}, u32[]{:S(2)}) copy-start(f32[128,4096]{1,0:T(8,128)} %get-tuple-element.18) | copy-start | bytes 6291460
  206.7 1.3 copy-start.3
  206.7 2.0 copy-start.2
  206.7 2.7 %copy-start.6 = (bf16[128,256]{1,0:T(8,128)(2,1)S(1)}, bf16[128,256]{1,0:T(8,128)(2,1)}, u32[]{:S(2)}) copy-start(bf16[128,256]{1,0:T(8,128)(2,1)} %get-tuple-element.37) | copy-start | bytes 196612
  206.7 3.3 %copy-start.5 = (bf16[128,256]{1,0:T(8,128)(2,1)S(1)}, bf16[128,256]{1,0:T(8,128)(2,1)}, u32[]{:S(2)}) copy-start(bf16[128,256]{1,0:T(8,128)(2,1)} %get-tuple-element.38) | copy-start | bytes 196612
  206.7 3.9 %copy-start.4 = (bf16[128,256]{1,0:T(8,128)(2,1)S(1)}, bf16[128,256]{1,0:T(8,128)(2,1)}, u32[]{:S(2)}) copy-start(bf16[128,256]{1,0:T(8,128)(2,1)} %get-tuple-element.39) | copy-start | bytes 196612

commit v2 on v1

--- a/solution.py
+++ b/solution.py
@@ -11,7 +11,8 @@
 BF = jnp.bfloat16
 F32 = jnp.float32
 MESH_ID = pl.DeviceIdType.MESH
-SUBS = 4
+SUBS = 2
+PIECES = 4
 
 
 def dot(a, b):
@@ -49,6 +50,8 @@
     wd,
     op,
     sent,
+    raw,
+    routed,
     acc_gu,
     acc_d,
     pick,
@@ -59,7 +62,14 @@
     part_out,
     part_in,
     run,
+    own_s,
     back,
+    side_out,
+    side_in,
+    group_out,
+    group_in,
+    far_out,
+    far_in,
     grad_gu,
     grad_d,
     full,
@@ -79,6 +89,12 @@
     g_recv,
     d_send,
     d_recv,
+    c_send,
+    c_recv,
+    q_send,
+    q_recv,
+    s_send,
+    s_recv,
     p_send,
     p_recv,
     r_send,
@@ -95,12 +111,18 @@
     h_recv,
     t_send,
     t_recv,
+    u_send,
+    u_recv,
+    v_send,
+    v_recv,
+    y_send,
+    y_recv,
 ):
     ny, nx, nz = dims
     ns = ny * nx
     hid, d_all = wg_hbm.shape
     toks, feat = state.shape
-    cap = sent.shape[2]
+    cap = sent.shape[1]
     slots = ns * cap
     y, x = lax.axis_index("y"), lax.axis_index("x")
     z, c = lax.axis_index("z"), lax.axis_index("c")
@@ -132,6 +154,9 @@
             device_id_type=MESH_ID,
         )
 
+    def half_cols(index, off):
+        return pl.ds(pl.multiple_of(index * feat + off, feat // 2), feat // 2)
+
     def cols(index):
         return pl.ds(pl.multiple_of(index * feat, feat), feat)
 
@@ -145,9 +170,40 @@
         load.start()
 
     barrier = pltpu.get_barrier_semaphore()
-    peers = [at_plane(dy, dx)[0] for dy, dx in shifts] + [on_z(up), on_z(down), partner]
+    peers = [at_plane(dy, dx)[0] for dy, dx in shifts] + [partner]
+    peers += [on_z(lax.rem(z + step, nz)) for step in range(1, nz)]
     for peer in peers:
         pl.semaphore_signal(barrier, inc=1, device_id=peer, device_id_type=MESH_ID)
+
+    pl.semaphore_wait(barrier, len(peers))
+
+    halves = toks // 2
+    hops = {(0, h): nz // 2 - h for h in range(2)} | {(1, h): nz // 2 - 1 + h for h in range(2)}
+
+    def along(way, k):
+        return lax.rem(z + nz - k, nz) if way == 0 else lax.rem(z + k, nz)
+
+    def raw_copy(way, h, k):
+        rows = pl.ds(h * halves, halves)
+        src = cot.at[rows] if k == 0 else raw.at[along(way, k), rows]
+        return remote(
+            src,
+            raw.at[along(way, k), rows],
+            c_send.at[way, h, k],
+            c_recv.at[way, h, k],
+            on_z(up if way == 0 else down),
+        )
+
+    def raw_wait(way, h, k):
+        part = raw.at[along(way, k), pl.ds(h * halves, halves)]
+        remote(
+            part, part, c_send.at[way, h, k - 1], c_recv.at[way, h, k - 1], partner
+        ).wait_recv()
+
+    for h in range(2):
+        for way in range(2):
+            if hops[(way, h)] > 0:
+                raw_copy(way, h, 0).start()
 
     expert = lax.broadcasted_iota(jnp.int32, (ns, toks), 0)
     first, second = ids[0:1, :] == expert, ids[1:2, :] == expert
@@ -167,35 +223,21 @@
         pick[pl.ds(e * cap, cap), :] = hit.astype(BF)
         scales.append(jnp.sum(hit * weight[e : e + 1, :], axis=1, keepdims=True))
     scale = jnp.concatenate(scales, axis=0)
-    sent[0] = dot(pick[...], state[...]).astype(BF).reshape(ns, cap, feat)
-    sent[1] = (dot(pick[...], cot[...]) * scale).astype(BF).reshape(ns, cap, feat)
-
-    pl.semaphore_wait(barrier, len(peers))
-
-    def route_copy(arr, index, dst_z, dev, s_to):
+    sent[...] = dot(pick[...], state[...]).astype(BF).reshape(ns, cap, feat)
+
+    def route_copy(index, dev, s_to):
         return remote(
-            sent.at[arr, s_to],
-            rows_all.at[arr, z, c, me],
-            a_send.at[arr, index],
-            a_recv.at[arr, me],
-            dev,
-        )
-
-    def route_wait(arr, s_from):
-        remote(
-            sent.at[arr, s_from],
-            rows_all.at[arr, z, c, s_from],
-            a_send.at[arr, 0],
-            a_recv.at[arr, s_from],
-            partner,
-        ).wait_recv()
+            sent.at[s_to], rows_all.at[0, z, c, me], a_send.at[index], a_recv.at[me], dev
+        )
+
+    def route_wait(s_from):
+        part = rows_all.at[0, z, c, s_from]
+        remote(part, part, a_send.at[0], a_recv.at[s_from], partner).wait_recv()
 
     for index, (dy, dx) in enumerate(shifts):
         dev, s_to = at_plane(dy, dx)
-        for arr in range(2):
-            route_copy(arr, index, z, dev, s_to).start()
-    for arr in range(2):
-        rows_all[arr, z, c, me] = sent[arr, me]
+        route_copy(index, dev, s_to).start()
+    rows_all[0, z, c, me] = sent[me]
 
     def rim_copy(arr, dev):
         src = (c_inner, c_input)[arr]
@@ -207,59 +249,121 @@
     for arr in range(2):
         rim_copy(arr, on_sp(following)).start()
 
+    def z_of(i):
+        step = lax.div(i + 1, 2)
+        return lax.rem(z + nz + step * (1 - 2 * lax.rem(i, 2)), nz)
+
+    def cot_copy(i, index, dev, s_to):
+        return remote(
+            routed.at[i, s_to],
+            rows_all.at[1, z_of(i), c, me],
+            q_send.at[i, index],
+            q_recv.at[i, me],
+            dev,
+        )
+
+    def cot_wait(i, s_from):
+        part = rows_all.at[1, z_of(i), c, s_from]
+        remote(part, part, q_send.at[i, 0], q_recv.at[i, s_from], partner).wait_recv()
+
+    def cot_route(i, rows):
+        picked = dot(pick[...], rows) * scale
+        routed[i] = picked.astype(BF).reshape(ns, cap, feat)
+        for index, (dy, dx) in enumerate(shifts):
+            dev, s_to = at_plane(dy, dx)
+            cot_copy(i, index, dev, s_to).start()
+        rows_all[1, z_of(i), c, me] = routed[i, me]
+
     acc_gu[...] = jnp.zeros_like(acc_gu)
     acc_d[...] = jnp.zeros_like(acc_d)
-    per_sub = ns // SUBS
-
-    def source_of(arr, t):
-        return lax.rem(z + nz - t, nz) if arr == 0 else lax.rem(z + t, nz)
-
-    def ring_copy(arr, sub, t):
-        part = rows_all.at[arr, source_of(arr, t), c, pl.ds(sub * per_sub, per_sub)]
+    half = slots // 2
+    ring_s = ns // 2
+    per_sub = ring_s // SUBS
+
+    def ring_copy(way, sub, t):
+        part = rows_all.at[0, along(way, t), c, pl.ds(way * ring_s + sub * per_sub, per_sub)]
         return remote(
             part,
             part,
-            g_send.at[arr, sub, t],
-            g_recv.at[arr, sub, t],
-            on_z(up if arr == 0 else down),
-        )
-
-    def ring_wait(arr, sub, t):
-        part = rows_all.at[arr, source_of(arr, t), c, pl.ds(sub * per_sub, per_sub)]
+            g_send.at[way, sub, t],
+            g_recv.at[way, sub, t],
+            on_z(up if way == 0 else down),
+        )
+
+    def ring_wait(way, sub, t):
+        part = rows_all.at[0, along(way, t), c, pl.ds(way * ring_s + sub * per_sub, per_sub)]
         remote(
-            part, part, g_send.at[arr, sub, t - 1], g_recv.at[arr, sub, t - 1], partner
+            part, part, g_send.at[way, sub, t - 1], g_recv.at[way, sub, t - 1], partner
         ).wait_recv()
 
-    def share(arr, t):
-        part = rows_all.at[arr, source_of(arr, t), c]
-        return remote(part, part, d_send.at[arr, t], d_recv.at[arr, t], partner)
-
-    def share_wait(arr, t):
-        part = rows_all.at[arr, source_of(arr, t), other]
-        remote(part, part, d_send.at[arr, t], d_recv.at[arr, t], partner).wait_recv()
-
-    def products(t):
-        for arr in range(2):
-            share_wait(arr, t)
+    def share(way, t, lane):
+        part = rows_all.at[0, along(way, t), lane, pl.ds(way * ring_s, ring_s)]
+        return remote(part, part, d_send.at[way, t], d_recv.at[way, t], partner)
+
+    def cot_share(i, lane):
+        part = rows_all.at[1, z_of(i), lane]
+        return remote(part, part, s_send.at[i], s_recv.at[i], partner)
+
+    def state_products(t):
+        for way in range(2):
+            share(way, t, other).wait_recv()
+        for way in range(2):
+            at = along(way, t)
+            for lane in range(2):
+                rows = rows_all[0, at, lane, way * ring_s : (way + 1) * ring_s]
+                acc_gu[way * half : (way + 1) * half, :] += dot_nt(
+                    rows.reshape(half, feat), wgu[:, cols(at * 2 + lane)]
+                )
+
+    def cot_products(i):
+        cot_share(i, other).wait_recv()
         for lane in range(2):
-            at = source_of(0, t)
-            rows = rows_all[0, at, lane].reshape(slots, feat)
-            acc_gu[...] += dot_nt(rows, wgu[:, cols(at * 2 + lane)])
-            at = source_of(1, t)
-            rows = rows_all[1, at, lane].reshape(slots, feat)
-            acc_d[...] += dot_nt(rows, wd[:, cols(at * 2 + lane)])
-
+            rows = rows_all[1, z_of(i), lane].reshape(slots, feat)
+            acc_d[...] += dot_nt(rows, wd[:, cols(z_of(i) * 2 + lane)])
+
+    def cot_arrived(i):
+        for dy, dx in shifts:
+            cot_wait(i, at_plane(dy, dx)[1])
+        cot_share(i, c).start()
+
+    cot_route(0, cot[...])
     for sub in range(SUBS):
-        for arr in range(2):
-            for s_from in range(sub * per_sub, (sub + 1) * per_sub):
+        for way in range(2):
+            first_s = way * ring_s + sub * per_sub
+            for s_from in range(first_s, first_s + per_sub):
 
                 @pl.when(s_from != me)
                 def _():
-                    route_wait(arr, s_from)
-
-            ring_copy(arr, sub, 0).start()
-    for arr in range(2):
-        share(arr, 0).start()
+                    route_wait(s_from)
+
+            ring_copy(way, sub, 0).start()
+    for way in range(2):
+        share(way, 0, c).start()
+    for load in loads:
+        load.wait()
+
+    def ring_step(t):
+        for sub in range(SUBS):
+            for way in range(2):
+                ring_wait(way, sub, t)
+
+                @pl.when(t < nz - 1)
+                def _():
+                    ring_copy(way, sub, t).start()
+
+        for way in range(2):
+            share(way, t, c).start()
+
+    for k in range(1, nz // 2 + 1):
+        for h in range(2):
+            for way in range(2):
+                if k <= hops[(way, h)]:
+                    raw_wait(way, h, k)
+                    if k < hops[(way, h)]:
+                        raw_copy(way, h, k).start()
+        cot_route(2 * k - 1, raw[along(0, k)])
+        if 2 * k < nz:
+            cot_route(2 * k, raw[along(1, k)])
 
     for arr in range(2):
         rim_copy(arr, on_sp(previous)).wait_recv()
@@ -267,33 +371,38 @@
     rim_prod = rim_in[0].astype(F32) * rim_in[1].astype(F32)
     rim_prod = jnp.where(me == 0, 0.0, rim_prod)
     ext = jnp.concatenate([rim_prod, inner * inp], axis=1)
-    n_taps = taps.shape[1]
-    conv_out = taps[:, n_taps - 1 : n_taps] * (inner * inp)
+    n_taps, chans = taps.shape
+    diagonal = lax.broadcasted_iota(jnp.int32, (chans, chans), 0) == lax.broadcasted_iota(
+        jnp.int32, (chans, chans), 1
+    )
+    tap = [
+        jnp.sum(jnp.where(diagonal, taps[j : j + 1, :], 0.0), axis=1, keepdims=True)
+        for j in range(n_taps)
+    ]
+    conv_out = tap[n_taps - 1] * (inner * inp)
     for j in range(n_taps - 1):
-        conv_out = conv_out + taps[:, j : j + 1] * pltpu.roll(ext, n_taps - 1 - j, 1)[:, 128:]
+        conv_out = conv_out + tap[j] * pltpu.roll(ext, n_taps - 1 - j, 1)[:, 128:]
     conv_s[...] = conv_out
     act_s[...] = (c_outer[...].astype(F32) * conv_out).astype(BF)
     pick_t[...] = pick[...].T
 
-    for load in loads:
-        load.wait()
-
-    def ring_step(t, carry):
-        for sub in range(SUBS):
-            for arr in range(2):
-                ring_wait(arr, sub, t)
-
-                @pl.when(t < nz - 1)
-                def _():
-                    ring_copy(arr, sub, t).start()
-
-        for arr in range(2):
-            share(arr, t).start()
-        products(t - 1)
+    def gather_step(t, carry):
+        ring_step(t)
+        cot_arrived(t - 1)
+        state_products(t - 1)
+
+        @pl.when(t > 1)
+        def _():
+            cot_products(t - 2)
+
         return carry
 
-    lax.fori_loop(1, nz, ring_step, 0)
-    products(nz - 1)
+    lax.fori_loop(1, nz, gather_step, 0)
+    cot_arrived(nz - 1)
+    state_products(nz - 1)
+    if nz > 1:
+        cot_products(nz - 2)
+    cot_products(nz - 1)
 
     gate_pre, up_pre = acc_gu[:, :hid], acc_gu[:, hid:]
     back_hidden = acc_d[...]
@@ -307,7 +416,6 @@
     bgu_t[:hid, :] = back_gate.T
     bgu_t[hid:, :] = back_up.T
 
-    half = slots // 2
     quarter = half // 2
 
     def target_of(way, t):
@@ -320,9 +428,60 @@
 
     def partner_part(t):
         for way in range(2):
-            w = wgu[:, cols(target_of(way, t) * 2 + other)]
+            w = wgu[:, half_cols(target_of(way, t) * 2 + other, 0)]
             part_out[way, t] = dot(bgu[pl.ds(way * half, half), :], w).astype(BF)
             part_copy(way, t).start()
+
+    n_groups = nz // 2
+    narrow = feat // 2
+
+    def z_of_side(j):
+        return lax.rem(lax.div(z, 2) + 1 + lax.div(j, 2), n_groups) * 2 + lax.rem(j, 2)
+
+    def side_copy(j):
+        return remote(side_out.at[j], side_in.at[j], u_send.at[j], u_recv.at[j], partner)
+
+    def side_part(j, carry):
+        w = wgu[:, half_cols(z_of_side(j) * 2 + other, narrow)]
+        side_out[j] = dot(bgu[...], w).astype(BF)
+        side_copy(j).start()
+        return carry
+
+    def group_copy(g, index, dev, s_to):
+        return remote(
+            group_out.at[g, s_to], group_in.at[g, me], v_send.at[g, index], v_recv.at[g, me], dev
+        )
+
+    def send_group(g):
+        for lane in range(2):
+            j = 2 * g + lane
+            side_copy(j).wait_recv()
+            w = wgu[:, half_cols(z_of_side(j) * 2 + c, narrow)]
+            total = dot(bgu[...], w) + side_in[j].astype(F32)
+            group_out[g, :, :, lane * narrow : (lane + 1) * narrow] = total.astype(BF).reshape(
+                ns, cap, narrow
+            )
+        for index, (dy, dx) in enumerate(shifts):
+            dev, s_to = at_plane(dy, dx)
+            group_copy(g, index, dev, s_to).start()
+        group_in[g, me] = group_out[g, me]
+
+    def far_copy(at):
+        return remote(far_out.at[at], far_in.at[z], y_send.at[at], y_recv.at[z], on_z(at))
+
+    def take_group(g):
+        for dy, dx in shifts:
+            s_from = at_plane(dy, dx)[1]
+            part = group_in.at[g, s_from]
+            remote(part, part, v_send.at[g, 0], v_recv.at[g, s_from], partner).wait_recv()
+        moved = dot(pick_t[...], group_in[g].reshape(slots, feat)).astype(BF)
+        for lane in range(2):
+            at = z_of_side(2 * g + lane)
+            far_out[at] = moved[:, lane * narrow : (lane + 1) * narrow]
+
+            @pl.when(at != z)
+            def _():
+                far_copy(at).start()
 
     def run_copy(way, sub, t):
         rows = pl.ds(sub * quarter, quarter)
@@ -335,37 +494,48 @@
         )
 
     for way in range(2):
-        run[way, 0] = jnp.zeros((half, feat), BF)
+        run[way, 0] = jnp.zeros((half, narrow), BF)
     partner_part(0)
+    lax.fori_loop(0, nz, side_part, 0)
 
     def reduce_step(t, carry):
+        for way in range(2):
+            part_copy(way, t).wait_recv()
+            w = wgu[:, half_cols(target_of(way, t) * 2 + c, 0)]
+            own = dot(bgu[pl.ds(way * half, half), :], w)
+            own_s[way] = own + part_in[way, t].astype(F32)
+        for sub in range(2):
+            for way in range(2):
+                rows = pl.ds(sub * quarter, quarter)
+
+                @pl.when(t > 0)
+                def _():
+                    run_copy(way, sub, t - 1).wait_recv()
+
+                total = own_s[way, rows] + run[way, t, rows].astype(F32)
+                run[way, t, rows] = total.astype(BF)
+
+                @pl.when(t < nz - 1)
+                def _():
+                    run_copy(way, sub, t).start()
+
         @pl.when(t < nz - 1)
         def _():
             partner_part(t + 1)
+
+        @pl.when(t < n_groups)
+        def _():
+            send_group(t)
 
         for lane in range(2):
             rows = rows_all[0, t, lane].reshape(slots, feat)
             grad_gu[:, cols(t * 2 + lane)] = dot(bgu_t[...], rows)
             rows = rows_all[1, t, lane].reshape(slots, feat)
             grad_d[:, cols(t * 2 + lane)] = dot(hid_t[...], rows)
-        for way in range(2):
-            part_copy(way, t).wait_recv()
-        for sub in range(2):
-            for way in range(2):
-                rows = pl.ds(sub * quarter, quarter)
-
-                @pl.when(t > 0)
-                def _():
-                    run_copy(way, sub, t - 1).wait_recv()
-
-                w = wgu[:, cols(target_of(way, t) * 2 + c)]
-                own = dot(bgu[pl.ds(way * half + sub * quarter, quarter), :], w)
-                total = own + part_in[way, t, rows].astype(F32) + run[way, t, rows].astype(F32)
-                run[way, t, rows] = total.astype(BF)
-
-                @pl.when(t < nz - 1)
-                def _():
-                    run_copy(way, sub, t).start()
+
+        @pl.when((t >= 3) & (lax.rem(t, 2) == 1))
+        def _():
+            take_group(lax.div(t - 3, 2))
 
         return carry
 
@@ -390,22 +560,27 @@
     back[me] = back_src(me)[...]
     for result in results:
         result.start()
+    for g in range(max(0, (nz - 2) // 2), n_groups):
+        take_group(g)
     for dy, dx in shifts:
         _, s_from = at_plane(dy, dx)
         remote(
             back_src(s_from), back.at[s_from], b_send.at[0], b_recv.at[s_from], partner
         ).wait_recv()
-    moe = dot(pick_t[...], back[...].reshape(slots, feat))
-    grad_mixed = (cot[...].astype(F32) + moe).astype(BF)
-    gm_out[...] = grad_mixed
+    moe = dot(pick_t[...], back[...].reshape(slots, narrow))
+    gm_out[:, :narrow] = (cot[:, :narrow].astype(F32) + moe).astype(BF)
+    moe = far_out[z].astype(F32)
+    for step in range(1, nz):
+        z_from = lax.rem(z + step, nz)
+        part = far_in.at[z_from]
+        remote(part, part, y_send.at[z_from], y_recv.at[z_from], partner).wait_recv()
+        moe = moe + far_in[z_from].astype(F32)
+    gm_out[:, narrow:] = (cot[:, narrow:].astype(F32) + moe).astype(BF)
+    grad_mixed = gm_out[...]
     full[z, c] = grad_mixed
 
-    halves = toks // 2
-    hops = {(0, h): nz // 2 - h for h in range(2)} | {(1, h): nz // 2 - 1 + h for h in range(2)}
-
     def full_part(way, h, k, lane):
-        at = lax.rem(z + nz - k, nz) if way == 0 else lax.rem(z + k, nz)
-        return full.at[at, lane, pl.ds(h * halves, halves)]
+        return full.at[along(way, k), lane, pl.ds(h * halves, halves)]
 
     def full_copy(way, h, k):
         part = full_part(way, h, k, c)
@@ -439,6 +614,19 @@
     for h in range(2):
         full_share(0, h, 0, c).start()
         shared.append((0, h, 0))
+    def proj_copy(index, dev, s_to):
+        return remote(proj_out.at[s_to], proj_in.at[me], j_send.at[index], j_recv.at[me], dev)
+
+    def proj_send(nearest, furthest):
+        for index, (dy, dx) in enumerate(shifts):
+            dev, s_to = at_plane(dy, dx)
+            off = lax.rem(lax.div(s_to, 2) + nz - z, nz)
+            far_enough = (off >= nearest) & (nz - off >= nearest)
+
+            @pl.when(far_enough & ((off <= furthest) | (nz - off <= furthest)))
+            def _():
+                proj_copy(index, dev, s_to).start()
+
     pending = [(0, [(0, 0, 0), (0, 1, 0)])]
     for k in range(1, nz // 2 + 1):
         news = {}
@@ -457,11 +645,14 @@
                 full_share(*args, other).wait_recv()
             mixer_products(lax.rem(z + nz - pos, nz))
         pending = list(news.items())
+        if k > 1:
+            proj_send(0 if k == 2 else k - 1, k - 1)
     for pos, waits in pending:
         for args in waits:
             full_share(*args, other).wait_recv()
         mixer_products(lax.rem(z + nz - pos, nz))
 
+    proj_send(nz // 2 if nz > 2 else 0, nz)
     back_mixer = bm_acc[...]
     back_conv = back_mixer * c_outer[...].astype(F32)
     tail_out[...] = back_conv[:, :128]
@@ -470,23 +661,16 @@
         return remote(tail_out, tail_in, t_send.at[0], t_recv.at[0], dev)
 
     tail_copy(on_sp(previous)).start()
-
-    def proj_copy(index, dev, s_to):
-        return remote(proj_out.at[s_to], proj_in.at[me], j_send.at[index], j_recv.at[me], dev)
-
-    for index, (dy, dx) in enumerate(shifts):
-        dev, s_to = at_plane(dy, dx)
-        proj_copy(index, dev, s_to).start()
 
     gouter[...] = (back_mixer * conv_s[...]).astype(BF)
     tail_copy(on_sp(following)).wait_recv()
     tail = jnp.where(me == ns - 1, 0.0, tail_in[...])
     ext = jnp.concatenate([back_conv, tail], axis=1)
     width = ext.shape[1]
-    back_prod = taps[:, n_taps - 1 : n_taps] * back_conv
+    back_prod = tap[n_taps - 1] * back_conv
     for j in range(n_taps - 1):
         back_prod = (
-            back_prod + taps[:, j : j + 1] * pltpu.roll(ext, width - (n_taps - 1 - j), 1)[:, :toks]
+            back_prod + tap[j] * pltpu.roll(ext, width - (n_taps - 1 - j), 1)[:, :toks]
         )
     ginner[...] = (back_prod * c_input[...].astype(F32)).astype(BF)
     ginput[...] = (back_prod * c_inner[...].astype(F32)).astype(BF)
@@ -504,8 +688,7 @@
         result.wait()
     for index, (dy, dx) in enumerate(shifts):
         dev, s_to = at_plane(dy, dx)
-        for arr in range(2):
-            route_copy(arr, index, z, dev, s_to).wait_send()
+        route_copy(index, dev, s_to).wait_send()
         back_copy(index, dev, s_to).wait_send()
         proj_copy(index, dev, s_to).wait_send()
     for arr in range(2):
@@ -523,17 +706,59 @@
     lax.fori_loop(0, nz - 1, ring_sent, 0)
 
     def shares_sent(t, carry):
-        for arr in range(2):
-            share(arr, t).wait_send()
-            part_copy(arr, t).wait_send()
+        for way in range(2):
+            share(way, t, c).wait_send()
+            part_copy(way, t).wait_send()
+        cot_share(t, c).wait_send()
+        side_copy(t).wait_send()
+        for index, (dy, dx) in enumerate(shifts):
+            dev, s_to = at_plane(dy, dx)
+            cot_copy(t, index, dev, s_to).wait_send()
         return carry
 
     lax.fori_loop(0, nz, shares_sent, 0)
+
+    def groups_sent(g, carry):
+        for index, (dy, dx) in enumerate(shifts):
+            dev, s_to = at_plane(dy, dx)
+            group_copy(g, index, dev, s_to).wait_send()
+        return carry
+
+    lax.fori_loop(0, n_groups, groups_sent, 0)
+    for step in range(1, nz):
+        far_copy(lax.rem(z + step, nz)).wait_send()
     for (way, h), n in hops.items():
         for k in range(n):
             full_copy(way, h, k).wait_send()
+            raw_copy(way, h, k).wait_send()
     for args in shared:
         full_share(*args, c).wait_send()
+
+
+def finish(*refs):
+    from_hbm, from_vmem = refs[0:3], refs[3:8]
+    to_hbm, to_vmem = refs[8:11], refs[11:16]
+    held, in_sem, out_sem = refs[16:19]
+    rows = from_hbm[0].shape[0] // PIECES
+
+    def copy_in(a, p):
+        part = pl.ds(p * rows, rows)
+        return pltpu.make_async_copy(from_hbm[a].at[part], held.at[a, part], in_sem.at[a, p])
+
+    def copy_out(a, p):
+        part = pl.ds(p * rows, rows)
+        return pltpu.make_async_copy(held.at[a, part], to_hbm[a].at[part], out_sem.at[a, p])
+
+    pieces = [(a, p) for a in range(3) for p in range(PIECES)]
+    for a, p in pieces:
+        copy_in(a, p).start()
+    for src, dst in zip(from_vmem, to_vmem):
+        dst[...] = src[...]
+    for a, p in pieces:
+        copy_in(a, p).wait()
+        copy_out(a, p).start()
+    for a, p in pieces:
+        copy_out(a, p).wait()
 
 
 def shards(
@@ -567,7 +792,9 @@
         pltpu.VMEM((2 * hid, d_all), BF),
         pltpu.VMEM((hid, d_all), BF),
         pltpu.VMEM((chans, d_all), BF),
-        pltpu.VMEM((2, ns, cap, feat), BF),
+        pltpu.VMEM((ns, cap, feat), BF),
+        pltpu.VMEM((nz, toks, feat), BF),
+        pltpu.VMEM((nz, ns, cap, feat), BF),
         pltpu.VMEM((slots, 2 * hid), F32),
         pltpu.VMEM((slots, hid), F32),
         pltpu.VMEM((slots, toks), BF),
@@ -575,10 +802,17 @@
         pltpu.VMEM((slots, 2 * hid), BF),
         pltpu.VMEM((2 * hid, slots), BF),
         pltpu.VMEM((hid, slots), BF),
-        pltpu.VMEM((2, nz, slots // 2, feat), BF),
-        pltpu.VMEM((2, nz, slots // 2, feat), BF),
-        pltpu.VMEM((2, nz, slots // 2, feat), BF),
-        pltpu.VMEM((ns, cap, feat), BF),
+        pltpu.VMEM((2, nz, slots // 2, feat // 2), BF),
+        pltpu.VMEM((2, nz, slots // 2, feat // 2), BF),
+        pltpu.VMEM((2, nz, slots // 2, feat // 2), BF),
+        pltpu.VMEM((2, slots // 2, feat // 2), F32),
+        pltpu.VMEM((ns, cap, feat // 2), BF),
+        pltpu.VMEM((nz, slots, feat // 2), BF),
+        pltpu.VMEM((nz, slots, feat // 2), BF),
+        pltpu.VMEM((nz // 2, ns, cap, feat), BF),
+        pltpu.VMEM((nz // 2, ns, cap, feat), BF),
+        pltpu.VMEM((nz, toks, feat // 2), BF),
+        pltpu.VMEM((nz, toks, feat // 2), BF),
         pltpu.VMEM((2 * hid, d_all), F32),
         pltpu.VMEM((hid, d_all), F32),
         pltpu.VMEM((nz, 2, toks, feat), BF),
@@ -592,12 +826,18 @@
         pltpu.VMEM((chans, toks), F32),
         dma((4,)),
         dma((3,)),
-        dma((2, ns)),
-        dma((2, ns)),
+        dma((ns,)),
+        dma((ns,)),
         dma((2, SUBS, nz)),
         dma((2, SUBS, nz)),
         dma((2, nz)),
         dma((2, nz)),
+        dma((2, 2, nz)),
+        dma((2, 2, nz)),
+        dma((nz, ns)),
+        dma((nz, ns)),
+        dma((nz,)),
+        dma((nz,)),
         dma((2, nz)),
         dma((2, nz)),
         dma((2, 2, nz)),
@@ -614,6 +854,12 @@
         dma((2,)),
         dma((1,)),
         dma((1,)),
+        dma((nz,)),
+        dma((nz,)),
+        dma((nz // 2, ns)),
+        dma((nz // 2, ns)),
+        dma((nz,)),
+        dma((nz,)),
     ]
     grad = jax.ShapeDtypeStruct((hid, d_all), F32)
     conv = jax.ShapeDtypeStruct((chans, toks), BF)
@@ -643,12 +889,20 @@
         conv_outer,
         conv_inner,
         conv_input,
-        conv_taps.T,
+        conv_taps,
         w_gate[0],
         w_up[0],
         w_down[0],
         out_proj,
     )
+    outs = pl.pallas_call(
+        finish,
+        out_shape=tuple(jax.ShapeDtypeStruct(o.shape, o.dtype) for o in outs),
+        in_specs=[hbm] * 3 + [vmem] * 5,
+        out_specs=(hbm,) * 3 + (vmem,) * 5,
+        scratch_shapes=[pltpu.VMEM((3, hid, d_all), F32), dma((3, PIECES)), dma((3, PIECES))],
+        compiler_params=pltpu.CompilerParams(vmem_limit_bytes=62000000),
+    )(*outs)
     return (outs[0][None], outs[1][None], outs[2][None], *outs[3:])
 
 

time: 214 us -> 175 us (0.82); the launches traced: 211 us -> 175 us
  Pallas kernels: 199 us -> 174 us
  local copies, waits for them, and re-layouts: 11.6 us -> 0 us
    pallas_call x1, Pallas kernels: 199 us -> 167 us  [shards(): pl.pallas_call(functools.partial(kernel, dims), out_shape=(grad, grad, gr...]
    unnamed x23 -> x0, local copies, waits for them, and re-layouts: 11.6 us -> none
    pallas_call x0 -> x1, Pallas kernels: none -> 7.25 us  [shards(): pl.pallas_call(finish, out_shape=tuple((jax.ShapeDtypeStruct(o.shape, o.d...]
where the time goes in v2:
time: 175 us
  Pallas kernels  174 us (99%)
    pallas_call x1, Pallas kernels, shards(): pl.pallas_call(functools.partial(kernel, dims), out_shape=(grad, grad, gr...  167 us
    pallas_call x1, Pallas kernels, shards(): pl.pallas_call(finish, out_shape=tuple((jax.ShapeDtypeStruct(o.shape, o.d...  7.25 us

profile of v2, /device:TPU:17, one launch (start us, length us, event | category | flops | bytes accessed | tf_op | source)
XLA Modules:
  0.0 175.2 jit_solution(10224258621377137209)
XLA Ops:
  0.6 167.1 %shard_map.179 = (f32[128,4096]{1,0:T(8,128)}, f32[128,4096]{1,0:T(8,128)}, f32[128,4096]{1,0:T(8,128)}, bf16[256,256]{1,0:T(8,128)(2,1)}, f32[128,256]{1,0:T(8,...) custom-call(s32[2,256]{1,0:T(2,128)} %bitcast.11, f32[2,256]{1,0:T(2,128)} %bitcast.12, ...), custom_call_target="tpu_custom_call" | custom-call | tf_op jit(solution)/shard_map/pallas_call | solution.py:866
  167.8 7.3 %shard_map.180 = (f32[128,4096]{1,0:T(8,128)}, f32[128,4096]{1,0:T(8,128)}, f32[128,4096]{1,0:T(8,128)}, bf16[256,256]{1,0:T(8,128)(2,1)}, f32[128,256]{1,0:T(8,...) custom-call(f32[128,4096]{1,0:T(8,128)} %get-tuple-element.24.refs_0_, ...), custom_call_target="tpu_custom_call" | custom-call | tf_op jit(solution)/shard_map/pallas_call | solution.py:898

commit v3 on v2

--- a/solution.py
+++ b/solution.py
@@ -13,6 +13,8 @@
 MESH_ID = pl.DeviceIdType.MESH
 SUBS = 2
 PIECES = 4
+EARLY = 3
+PARTS = 4
 
 
 def dot(a, b):
@@ -177,8 +179,11 @@
 
     pl.semaphore_wait(barrier, len(peers))
 
-    halves = toks // 2
-    hops = {(0, h): nz // 2 - h for h in range(2)} | {(1, h): nz // 2 - 1 + h for h in range(2)}
+    halves = toks // PARTS
+    hops = {}
+    for h in range(PARTS):
+        late = 2 * h // PARTS
+        hops[(0, h)], hops[(1, h)] = nz // 2 - late, nz // 2 - 1 + late
 
     def along(way, k):
         return lax.rem(z + nz - k, nz) if way == 0 else lax.rem(z + k, nz)
@@ -200,7 +205,7 @@
             part, part, c_send.at[way, h, k - 1], c_recv.at[way, h, k - 1], partner
         ).wait_recv()
 
-    for h in range(2):
+    for h in range(PARTS):
         for way in range(2):
             if hops[(way, h)] > 0:
                 raw_copy(way, h, 0).start()
@@ -326,7 +331,6 @@
             cot_wait(i, at_plane(dy, dx)[1])
         cot_share(i, c).start()
 
-    cot_route(0, cot[...])
     for sub in range(SUBS):
         for way in range(2):
             first_s = way * ring_s + sub * per_sub
@@ -339,6 +343,7 @@
             ring_copy(way, sub, 0).start()
     for way in range(2):
         share(way, 0, c).start()
+    cot_route(0, cot[...])
     for load in loads:
         load.wait()
 
@@ -355,7 +360,7 @@
             share(way, t, c).start()
 
     for k in range(1, nz // 2 + 1):
-        for h in range(2):
+        for h in range(PARTS):
             for way in range(2):
                 if k <= hops[(way, h)]:
                     raw_wait(way, h, k)
@@ -364,6 +369,8 @@
         cot_route(2 * k - 1, raw[along(0, k)])
         if 2 * k < nz:
             cot_route(2 * k, raw[along(1, k)])
+        if k < min(nz, EARLY + 1):
+            ring_step(k)
 
     for arr in range(2):
         rim_copy(arr, on_sp(previous)).wait_recv()
@@ -387,7 +394,10 @@
     pick_t[...] = pick[...].T
 
     def gather_step(t, carry):
-        ring_step(t)
+        @pl.when(t > EARLY)
+        def _():
+            ring_step(t)
+
         cot_arrived(t - 1)
         state_products(t - 1)
 
@@ -441,11 +451,10 @@
     def side_copy(j):
         return remote(side_out.at[j], side_in.at[j], u_send.at[j], u_recv.at[j], partner)
 
-    def side_part(j, carry):
+    def side_part(j):
         w = wgu[:, half_cols(z_of_side(j) * 2 + other, narrow)]
         side_out[j] = dot(bgu[...], w).astype(BF)
         side_copy(j).start()
-        return carry
 
     def group_copy(g, index, dev, s_to):
         return remote(
@@ -496,7 +505,8 @@
     for way in range(2):
         run[way, 0] = jnp.zeros((half, narrow), BF)
     partner_part(0)
-    lax.fori_loop(0, nz, side_part, 0)
+    side_part(0)
+    side_part(1)
 
     def reduce_step(t, carry):
         for way in range(2):
@@ -527,15 +537,20 @@
         def _():
             send_group(t)
 
+        @pl.when(t < n_groups - 1)
+        def _():
+            side_part(2 * t + 2)
+            side_part(2 * t + 3)
+
         for lane in range(2):
             rows = rows_all[0, t, lane].reshape(slots, feat)
             grad_gu[:, cols(t * 2 + lane)] = dot(bgu_t[...], rows)
             rows = rows_all[1, t, lane].reshape(slots, feat)
             grad_d[:, cols(t * 2 + lane)] = dot(hid_t[...], rows)
 
-        @pl.when((t >= 3) & (lax.rem(t, 2) == 1))
+        @pl.when((t >= 2) & (lax.rem(t, 2) == 0))
         def _():
-            take_group(lax.div(t - 3, 2))
+            take_group(lax.div(t - 2, 2))
 
         return carry
 
@@ -607,11 +622,11 @@
             proj_out[at * 2 + lane] = dot(act_s[...], f).astype(BF)
 
     shared = []
-    for h in range(2):
+    for h in range(PARTS):
         for way in range(2):
             if hops[(way, h)] > 0:
                 full_copy(way, h, 0).start()
-    for h in range(2):
+    for h in range(PARTS):
         full_share(0, h, 0, c).start()
         shared.append((0, h, 0))
     def proj_copy(index, dev, s_to):
@@ -627,10 +642,10 @@
             def _():
                 proj_copy(index, dev, s_to).start()
 
-    pending = [(0, [(0, 0, 0), (0, 1, 0)])]
+    pending = [(0, [(0, h, 0) for h in range(PARTS)])]
     for k in range(1, nz // 2 + 1):
         news = {}
-        for h in range(2):
+        for h in range(PARTS):
             for way in range(2):
                 if k > hops[(way, h)]:
                     continue
@@ -652,19 +667,20 @@
             full_share(*args, other).wait_recv()
         mixer_products(lax.rem(z + nz - pos, nz))
 
-    proj_send(nz // 2 if nz > 2 else 0, nz)
     back_mixer = bm_acc[...]
     back_conv = back_mixer * c_outer[...].astype(F32)
-    tail_out[...] = back_conv[:, :128]
+    tail_out[...] = back_conv[:, :128].T[:8, :]
 
     def tail_copy(dev):
         return remote(tail_out, tail_in, t_send.at[0], t_recv.at[0], dev)
 
     tail_copy(on_sp(previous)).start()
+    proj_send(nz // 2 if nz > 2 else 0, nz)
 
     gouter[...] = (back_mixer * conv_s[...]).astype(BF)
     tail_copy(on_sp(following)).wait_recv()
-    tail = jnp.where(me == ns - 1, 0.0, tail_in[...])
+    tail = jnp.concatenate([tail_in[...], jnp.zeros((120, tail_in.shape[1]), F32)], axis=0).T
+    tail = jnp.where(me == ns - 1, 0.0, tail)
     ext = jnp.concatenate([back_conv, tail], axis=1)
     width = ext.shape[1]
     back_prod = tap[n_taps - 1] * back_conv
@@ -819,8 +835,8 @@
         pltpu.VMEM((nz * 2, chans, feat), BF),
         pltpu.VMEM((ns, chans, feat), BF),
         pltpu.VMEM((2, chans, 128), BF),
-        pltpu.VMEM((chans, 128), F32),
-        pltpu.VMEM((chans, 128), F32),
+        pltpu.VMEM((8, chans), F32),
+        pltpu.VMEM((8, chans), F32),
         pltpu.VMEM((chans, toks), F32),
         pltpu.VMEM((chans, toks), BF),
         pltpu.VMEM((chans, toks), F32),
@@ -832,8 +848,8 @@
         dma((2, SUBS, nz)),
         dma((2, nz)),
         dma((2, nz)),
-        dma((2, 2, nz)),
-        dma((2, 2, nz)),
+        dma((2, PARTS, nz)),
+        dma((2, PARTS, nz)),
         dma((nz, ns)),
         dma((nz, ns)),
         dma((nz,)),
@@ -844,10 +860,10 @@
         dma((2, 2, nz)),
         dma((ns,)),
         dma((ns,)),
-        dma((2, 2, nz)),
-        dma((2, 2, nz)),
-        dma((2, 2, nz)),
-        dma((2, 2, nz)),
+        dma((2, PARTS, nz)),
+        dma((2, PARTS, nz)),
+        dma((2, PARTS, nz)),
+        dma((2, PARTS, nz)),
         dma((ns,)),
         dma((ns,)),
         dma((2,)),

time: 175 us -> 183 us (1.046)
  Pallas kernels: 174 us -> 182 us
    pallas_call x1, Pallas kernels: 167 us -> 174 us  [shards(): pl.pallas_call(functools.partial(kernel, dims), out_shape=(grad, grad, gr...]
where the time goes in v3:
time: 183 us; the launch traced here: 182 us
  Pallas kernels  182 us (99%)
    pallas_call x1, Pallas kernels, shards(): pl.pallas_call(functools.partial(kernel, dims), out_shape=(grad, grad, gr...  174 us
    pallas_call x1, Pallas kernels, shards(): pl.pallas_call(finish, out_shape=tuple((jax.ShapeDtypeStruct(o.shape, o.d...  7.25 us

profile of v3, /device:TPU:17, one launch (start us, length us, event | category | flops | bytes accessed | tf_op | source)
XLA Modules:
  0.0 182.4 jit_solution(7535003458665795628)
XLA Ops:
  0.6 174.4 %shard_map.179 = (f32[128,4096]{1,0:T(8,128)}, f32[128,4096]{1,0:T(8,128)}, f32[128,4096]{1,0:T(8,128)}, bf16[256,256]{1,0:T(8,128)(2,1)}, f32[128,256]{1,0:T(8,...) custom-call(s32[2,256]{1,0:T(2,128)} %bitcast.11, f32[2,256]{1,0:T(2,128)} %bitcast.12, ...), custom_call_target="tpu_custom_call" | custom-call | tf_op jit(solution)/shard_map/pallas_call | solution.py:882
  175.0 7.3 %shard_map.180 = (f32[128,4096]{1,0:T(8,128)}, f32[128,4096]{1,0:T(8,128)}, f32[128,4096]{1,0:T(8,128)}, bf16[256,256]{1,0:T(8,128)(2,1)}, f32[128,256]{1,0:T(8,...) custom-call(f32[128,4096]{1,0:T(8,128)} %get-tuple-element.24.refs_0_, ...), custom_call_target="tpu_custom_call" | custom-call | tf_op jit(solution)/shard_map/pallas_call | solution.py:914
